TPU v7x, 32 devices: a whole 2x2x4 slice. The times are simulated.
32 devices in a mesh: sp: 8 (over z, x), dp: 4 (over y, core).
Axes of the slice: x: 2, y: 2, z: 4, core: 2. Of those that a mesh axis runs over, the one named last changes fastest.
Arguments:
- queries: bfloat16 [4, 1024, 16, 128], P('dp', 'sp'), may hold values from -3.5 to 2
- key_rows: bfloat16 [4, 1024, 16, 128], P('dp', 'sp'), may hold values from -4 to 5.3
- values: bfloat16 [4, 1024, 16, 128], P('dp', 'sp'), may hold values from -6 to 6
- residual: bfloat16 [4, 1024, 4096], P('dp', 'sp'), may hold values from -6 to 6
- out_weight: bfloat16 [2048, 4096], P(None, 'dp'), may hold values from -0.125 to 0.125
- mixer_gain: float32 [4096], replicated, may hold values from 0.1 to 1.9
- expert_gain: float32 [4096], replicated, may hold values from 0.1 to 1.9
- gate_weight: bfloat16 [32, 4096, 512], P(('sp', 'dp')), may hold values from -0.09375 to 0.09375
- up_weight: bfloat16 [32, 4096, 512], P(('sp', 'dp')), may hold values from -0.09375 to 0.09375
- expert_down_matrix: bfloat16 [32, 512, 4096], P(('sp', 'dp')), may hold values from -0.25 to 0.25
- routes: int32 [4, 1024, 2], P('dp', 'sp'), may hold values from 0 to 31, all different within a row; in each aligned block of 128 rows (0 to 127, 128 to 255, ..., all dimensions but the last counted through in order) at most 12 rows name the same one
- route_weight: float32 [4, 1024, 2], P('dp', 'sp'), may hold values from 0.1 to 1
- output_gain: float32 [4096], replicated, may hold values from 0.1 to 1.9
Outputs:
- output: bfloat16 [4, 1024, 4096], P('dp', 'sp')
Inputs may be any that keep to these rules, and one draw needn't show every extreme that they name: `routes`: each row names 2 different experts. Among the rows of one device no expert is named more than 12 times, and in every draw some device names some expert exactly 12 times.
All inputs are finite; a program needn't handle non-finite values.
Results may differ from a plain program's by a relative error of at most 0.009.
Values may be sent and summed in bfloat16 or wider, within the bound.
A program may use at most 192 MiB of HBM per device.

v0:
```python
import functools

import jax
import jax.numpy as jnp
from jax import lax
from jax.experimental import pallas as pl
from jax.experimental.pallas import tpu as pltpu
from jax.sharding import PartitionSpec as P

EPSILON = 1e-06
MESH = pl.DeviceIdType.MESH
VMEM_LIMIT = 56 * 1024 * 1024


def normed_token_rows(matrix, gain):
    return matrix * lax.rsqrt(jnp.mean(matrix * matrix, axis=-1, keepdims=True) + EPSILON) * gain


def peer_id(axes, sizes, flat):
    if len(axes) == 1:
        return {axes[0]: flat}
    return {axes[0]: lax.div(flat, sizes[1]), axes[1]: lax.rem(flat, sizes[1])}


def exchange_kernel(axes, sizes, n, count, *refs):
    ins, outs = refs[:count], refs[count : 2 * count]
    stages = refs[2 * count : 3 * count]
    send_sem, recv_sem, local_sem = refs[3 * count :]
    me = lax.axis_index(axes[0])
    if len(axes) == 2:
        me = me * sizes[1] + lax.axis_index(axes[1])

    barrier = pltpu.get_barrier_semaphore()

    def greet(k, carry):
        pl.semaphore_signal(
            barrier, inc=1, device_id=peer_id(axes, sizes, lax.rem(me + k, n)), device_id_type=MESH
        )
        return carry

    lax.fori_loop(1, n, greet, 0)
    loads = [
        pltpu.make_async_copy(ins[a].at[me], stages[a], local_sem.at[a]) for a in range(count)
    ]
    for load in loads:
        load.start()
    pl.semaphore_wait(barrier, n - 1)

    def copies(k):
        target = lax.rem(me + k, n)
        return [
            pltpu.make_async_remote_copy(
                src_ref=ins[a].at[target],
                dst_ref=outs[a].at[me],
                send_sem=send_sem.at[a, k],
                recv_sem=recv_sem.at[a, k],
                device_id=peer_id(axes, sizes, target),
                device_id_type=MESH,
            )
            for a in range(count)
        ]

    def push(i, carry):
        k = n // 2 + (1 - 2 * lax.rem(i, 2)) * lax.div(i + 1, 2)
        for copy in copies(k):
            copy.start()
        return carry

    lax.fori_loop(0, n - 1, push, 0)
    stores = [
        pltpu.make_async_copy(stages[a], outs[a].at[me], local_sem.at[a]) for a in range(count)
    ]
    for load in loads:
        load.wait()
    for store in stores:
        store.start()
    for store in stores:
        store.wait()

    def finish(k, carry):
        for copy in copies(k):
            copy.wait()
        return carry

    lax.fori_loop(1, n, finish, 0)


def exchange(arrays, axes, collective_id):
    sizes = [lax.axis_size(a) for a in axes]
    n = arrays[0].shape[0]
    count = len(arrays)
    moved = sum(a.size * 2 for a in arrays)
    return pl.pallas_call(
        functools.partial(exchange_kernel, axes, sizes, n, count),
        out_shape=[jax.ShapeDtypeStruct(a.shape, a.dtype) for a in arrays],
        in_specs=[pl.BlockSpec(memory_space=pl.ANY)] * count,
        out_specs=[pl.BlockSpec(memory_space=pl.ANY)] * count,
        scratch_shapes=[pltpu.VMEM(a.shape[1:], a.dtype) for a in arrays]
        + [
            pltpu.SemaphoreType.DMA((count, n)),
            pltpu.SemaphoreType.DMA((count, n)),
            pltpu.SemaphoreType.DMA((count,)),
        ],
        compiler_params=pltpu.CompilerParams(
            collective_id=collective_id, has_side_effects=True, vmem_limit_bytes=VMEM_LIMIT
        ),
        cost_estimate=pl.CostEstimate(flops=0, bytes_accessed=moved * 20, transcendentals=0),
    )(*arrays)


def attend_kernel(block, q_ref, k_ref, v_ref, out_ref):
    sources, _, rows, width = q_ref.shape
    length = sources * rows
    scale = width ** (-0.5)
    tri_row = lax.broadcasted_iota(jnp.int32, (block, block), 0)
    tri_col = lax.broadcasted_iota(jnp.int32, (block, block), 1)
    suffix_ones = (tri_row >= tri_col).astype(jnp.bfloat16)
    is_past = tri_col < tri_row
    per = block // rows

    def piece(ref, index):
        return ref[index * per : (index + 1) * per, 0].reshape(block, width)

    for q_block in range(length // block):
        query = piece(q_ref, q_block)
        total = jnp.zeros((block, width), jnp.float32)
        later = jnp.zeros((block, 1), jnp.float32)
        for k_block in range(q_block, -1, -1):
            scores = (
                lax.dot_general(
                    query,
                    piece(k_ref, k_block),
                    (((1,), (1,)), ((), ())),
                    preferred_element_type=jnp.float32,
                )
                * scale
            )
            soft = jnp.maximum(scores, 0.0) + jnp.log(1.0 + jnp.exp(-jnp.abs(scores)))
            if k_block == q_block:
                soft = jnp.where(is_past, soft, 0.0)
            high = soft.astype(jnp.bfloat16)
            low = (soft - high.astype(jnp.float32)).astype(jnp.bfloat16)
            suffix = jnp.dot(high, suffix_ones, preferred_element_type=jnp.float32) + jnp.dot(
                low, suffix_ones, preferred_element_type=jnp.float32
            )
            weights = jnp.exp(scores - suffix - later)
            if k_block == q_block:
                weights = jnp.where(is_past, weights, 0.0)
            total = total + jnp.dot(
                weights.astype(jnp.bfloat16),
                piece(v_ref, k_block),
                preferred_element_type=jnp.float32,
            )
            if k_block > 0:
                later = later + suffix[:, :1]
        out_ref[q_block * per : (q_block + 1) * per, 0] = total.astype(jnp.bfloat16).reshape(
            per, rows, width
        )


def attend(query, key, value):
    sources, heads, rows, width = query.shape
    block = rows * max(1, min(sources, 256 // rows))
    spec = pl.BlockSpec((sources, 1, rows, width), lambda h: (0, h, 0, 0))
    return pl.pallas_call(
        functools.partial(attend_kernel, block),
        grid=(heads,),
        out_shape=jax.ShapeDtypeStruct(query.shape, jnp.bfloat16),
        in_specs=[spec] * 3,
        out_specs=spec,
        compiler_params=pltpu.CompilerParams(vmem_limit_bytes=VMEM_LIMIT),
        cost_estimate=pl.CostEstimate(
            flops=6 * heads * (sources * rows) ** 2 * width, bytes_accessed=8 * query.size, transcendentals=0
        ),
    )(query, key, value)


def project_kernel(attn_ref, weight_ref, out_ref):
    for part in range(attn_ref.shape[0]):
        flat = jnp.concatenate([attn_ref[part, h] for h in range(attn_ref.shape[1])], axis=1)
        out_ref[part] = jnp.dot(
            flat, weight_ref[...], preferred_element_type=jnp.float32
        ).astype(jnp.bfloat16)


def project(attn, weight):
    parts, _, rows, _ = attn.shape
    return pl.pallas_call(
        project_kernel,
        out_shape=jax.ShapeDtypeStruct((parts, rows, weight.shape[1]), jnp.bfloat16),
        in_specs=[pl.BlockSpec(memory_space=pltpu.VMEM)] * 2,
        out_specs=pl.BlockSpec(memory_space=pltpu.VMEM),
        compiler_params=pltpu.CompilerParams(vmem_limit_bytes=VMEM_LIMIT),
    )(attn, weight)


def mix_kernel(parts_ref, resid_ref, mixer_ref, expert_ref, pick_ref, stream_ref, *sent_refs):
    projected = jnp.concatenate(
        [parts_ref[part].astype(jnp.float32) for part in range(parts_ref.shape[0])], axis=1
    )
    stream = (
        resid_ref[...].astype(jnp.float32) + normed_token_rows(projected, mixer_ref[...])
    ).astype(jnp.bfloat16)
    stream_ref[...] = stream
    tokens = normed_token_rows(stream.astype(jnp.float32), expert_ref[...]).astype(jnp.bfloat16)
    row = 0
    for ref in sent_refs:
        many = ref.shape[0]
        ref[...] = jnp.dot(
            pick_ref[row : row + many], tokens, preferred_element_type=jnp.float32
        ).astype(jnp.bfloat16)
        row += many


def mix(parts, residual, mixer_gain, expert_gain, pick, splits):
    rows, features = residual.shape
    return pl.pallas_call(
        mix_kernel,
        out_shape=[jax.ShapeDtypeStruct((many, features), jnp.bfloat16) for many in [rows] + splits],
        in_specs=[pl.BlockSpec(memory_space=pltpu.VMEM)] * 5,
        out_specs=[pl.BlockSpec(memory_space=pltpu.VMEM)] * (1 + len(splits)),
        compiler_params=pltpu.CompilerParams(vmem_limit_bytes=VMEM_LIMIT),
    )(parts, residual, mixer_gain[None], expert_gain[None], pick)


def expert_kernel(count, *refs):
    ins, (gate_ref, up_ref, down_ref) = refs[:count], refs[count : count + 3]
    outs = refs[count + 3 :]
    for a in range(count):
        rows = ins[a][...]
        gate = jnp.dot(rows, gate_ref[...], preferred_element_type=jnp.float32)
        upward = jnp.dot(rows, up_ref[...], preferred_element_type=jnp.float32)
        hidden = (gate / (1.0 + jnp.exp(-gate)) * upward).astype(jnp.bfloat16)
        outs[a][...] = jnp.dot(
            hidden, down_ref[...], preferred_element_type=jnp.float32
        ).astype(jnp.bfloat16)


def serve(arrays, gate, up, down):
    return pl.pallas_call(
        functools.partial(expert_kernel, len(arrays)),
        out_shape=[jax.ShapeDtypeStruct(a.shape, a.dtype) for a in arrays],
        in_specs=[pl.BlockSpec(memory_space=pltpu.VMEM)] * (len(arrays) + 3),
        out_specs=[pl.BlockSpec(memory_space=pltpu.VMEM)] * len(arrays),
        compiler_params=pltpu.CompilerParams(vmem_limit_bytes=VMEM_LIMIT),
    )(*arrays, gate, up, down)


def combine_kernel(count, *refs):
    ins = refs[:count]
    high_ref, low_ref, stream_ref, gain_ref, out_ref = refs[count:]
    combined, row = 0.0, 0
    for ref in ins:
        many = ref.shape[0]
        for share in (high_ref, low_ref):
            combined = combined + jnp.dot(
                share[:, row : row + many], ref[...], preferred_element_type=jnp.float32
            )
        row += many
    out_ref[...] = (
        stream_ref[...].astype(jnp.float32) + normed_token_rows(combined, gain_ref[...])
    ).astype(jnp.bfloat16)


def combine(arrays, high, low, stream, gain):
    return pl.pallas_call(
        functools.partial(combine_kernel, len(arrays)),
        out_shape=jax.ShapeDtypeStruct(stream.shape, jnp.bfloat16),
        in_specs=[pl.BlockSpec(memory_space=pltpu.VMEM)] * (len(arrays) + 4),
        out_specs=pl.BlockSpec(memory_space=pltpu.VMEM),
        compiler_params=pltpu.CompilerParams(vmem_limit_bytes=VMEM_LIMIT),
    )(*arrays, high, low, stream, gain[None])


def local(
    queries,
    key_rows,
    values,
    residual,
    out_weight,
    mixer_gain,
    expert_gain,
    gate_weight,
    up_weight,
    expert_down_matrix,
    routes,
    route_weight,
    output_gain,
):
    sp = lax.axis_size("sp")
    _, local_rows, heads, width = queries.shape
    features = residual.shape[2]

    def by_head(tensor):
        return jnp.transpose(tensor[0], (1, 0, 2)).reshape(sp, heads // sp, local_rows, width)

    head_parts = exchange([by_head(queries), by_head(key_rows), by_head(values)], ("sp",), 0)
    attended = attend(*head_parts)
    (token_parts,) = exchange([attended], ("sp",), 1)

    dp = lax.axis_size("dp")
    token_heads = token_parts.reshape(heads, local_rows, width)
    (group_heads,) = exchange([jnp.broadcast_to(token_heads[None], (dp,) + token_heads.shape)], ("dp",), 4)
    (projected_parts,) = exchange([project(group_heads, out_weight)], ("dp",), 5)

    experts = sp * dp
    top_count = routes.shape[2]
    capacity = max(2, 3 * local_rows // experts)
    picked = routes[0].reshape(local_rows * top_count)
    onehot = (
        picked[:, None] == lax.broadcasted_iota(jnp.int32, (picked.shape[0], experts), 1)
    ).astype(jnp.bfloat16)
    count = picked.shape[0]
    earlier = (
        lax.broadcasted_iota(jnp.int32, (count, count), 1)
        < lax.broadcasted_iota(jnp.int32, (count, count), 0)
    ).astype(jnp.bfloat16)
    before = jnp.dot(earlier, onehot, preferred_element_type=jnp.float32)
    rank = jnp.sum(before * onehot.astype(jnp.float32), axis=1).astype(jnp.int32)
    groups = [g for g in (capacity // 8 * 8, capacity % 8) if g]
    splits = [g * experts for g in groups]
    slot, first, base = jnp.full((count,), -1, jnp.int32), 0, 0
    for g in groups:
        inside = (rank >= first) & (rank < first + g)
        slot = jnp.where(inside, base + picked * g + rank - first, slot)
        first, base = first + g, base + g * experts
    slot = slot.reshape(local_rows, top_count)
    slot_ids = lax.broadcasted_iota(jnp.int32, (local_rows, base), 1)
    hits = [slot[:, k : k + 1] == slot_ids for k in range(top_count)]
    pick = functools.reduce(jnp.logical_or, hits).astype(jnp.bfloat16).T
    share = sum(jnp.where(hits[k], route_weight[0][:, k : k + 1], 0.0) for k in range(top_count))
    share_high = share.astype(jnp.bfloat16)
    share_low = (share - share_high.astype(jnp.float32)).astype(jnp.bfloat16)

    stream, *outgoing = mix(
        projected_parts,
        residual[0],
        mixer_gain,
        expert_gain,
        pick,
        splits,
    )

    def blocks(arrays):
        return [a.reshape(experts, g, features) for a, g in zip(arrays, groups)]

    def flat(arrays):
        return [a.reshape(-1, features) for a in arrays]

    arrived = exchange(blocks(outgoing), ("sp", "dp"), 2)
    results = serve(flat(arrived), gate_weight[0], up_weight[0], expert_down_matrix[0])
    returned = exchange(blocks(results), ("sp", "dp"), 3)
    output = combine(flat(returned), share_high, share_low, stream, output_gain)
    return output[None]


def solution(mesh):
    in_specs = (
        P("dp", "sp", None, None),
        P("dp", "sp", None, None),
        P("dp", "sp", None, None),
        P("dp", "sp", None),
        P(None, "dp"),
        P(),
        P(),
        P(("sp", "dp"), None, None),
        P(("sp", "dp"), None, None),
        P(("sp", "dp"), None, None),
        P("dp", "sp", None),
        P("dp", "sp", None),
        P(),
    )
    out_specs = P("dp", "sp", None)
    return jax.shard_map(local, mesh=mesh, in_specs=in_specs, out_specs=out_specs, check_vma=False)
```

profile of v0, /device:TPU:16, one launch (start us, length us, event | category | flops | bytes accessed | tf_op | source)
XLA Modules:
  0.0 306.9 jit_solution(3955832125532476193)
XLA Ops:
  0.0 0.0 copy-start
  0.0 2.0 copy.31
  2.0 2.0 copy.32
  4.0 0.0 copy-done
  4.0 0.9 copy.33
  5.0 38.9 %shard_map.127 = (bf16[8,2,128,128]{3,2,1,0:T(8,128)(2,1)}, bf16[8,2,128,128]{3,2,1,0:T(8,128)(2,1)}, bf16[8,2,128,128]{3,2,1,0:T(8,128)(2,1)}) custom-call(bf16[8,2,128,128]{3,2,1,0:T(8,128)(2,1)} %bitcast.48, bf16[8,2,128,128]{3,2,1,0:T(8,128)(2,1)} %bitcast.49, bf16[8,2,128,128]{3,2,1,0:T(8,128)(2,1)} %bitcast.50), custom_call_target="tpu_custom_call" | custom-call | bytes 31457280 | tf_op jit(solution)/shard_map/pallas_call | solution.py:93
  43.9 8.6 %shard_map.128.refs_0_ = bf16[8,2,128,128]{3,2,1,0:T(8,128)(2,1)} custom-call(bf16[8,2,128,128]{3,2,1,0:T(8,128)(2,1)} %get-tuple-element.17.q_ref, bf16[8,2,128,128]{3,2,1,0:T(8,128)(2,1)} %get-tuple-element.18.k_ref, bf16[8,2,128,128]{3,2,1,0:T(8,128)(2,1)} %get-tuple-element.19.v_ref), custom_call_target="tpu_custom_call" | custom-call | flops 1610612736 | bytes 2097152 | tf_op jit(solution)/shard_map/pallas_call | solution.py:165
  52.5 14.3 %shard_map.129 = bf16[8,2,128,128]{3,2,1,0:T(8,128)(2,1)} custom-call(bf16[8,2,128,128]{3,2,1,0:T(8,128)(2,1)} %shard_map.128.refs_0_), custom_call_target="tpu_custom_call" | custom-call | bytes 10485760 | tf_op jit(solution)/shard_map/pallas_call | solution.py:93
  66.8 2.9 broadcast_in_dim.45.refs_0_
  69.7 25.3 %shard_map.130.attn_ref = bf16[4,16,128,128]{3,2,1,0:T(8,128)(2,1)} custom-call(bf16[4,16,128,128]{3,2,1,0:T(8,128)(2,1)} %broadcast_in_dim.45.refs_0_), custom_call_target="tpu_custom_call" | custom-call | bytes 41943040 | tf_op jit(solution)/shard_map/pallas_call | solution.py:93
  95.0 6.1 %shard_map.131.refs_0_ = bf16[4,128,1024]{2,1,0:T(8,128)(2,1)} custom-call(bf16[4,16,128,128]{3,2,1,0:T(8,128)(2,1)} %shard_map.130.attn_ref, bf16[2048,1024]{1,0:T(8,128)(2,1)} %weight_ref.1), custom_call_target="tpu_custom_call" | custom-call | tf_op jit(solution)/shard_map/pallas_call | solution.py:188
  101.1 0.0 copy-start.1
  101.1 14.0 %shard_map.132.parts_ref = bf16[4,128,1024]{2,1,0:T(8,128)(2,1)} custom-call(bf16[4,128,1024]{2,1,0:T(8,128)(2,1)} %shard_map.131.refs_0_), custom_call_target="tpu_custom_call" | custom-call | bytes 20971520 | tf_op jit(solution)/shard_map/pallas_call | solution.py:93
  115.2 0.0 copy-done.1
  115.2 0.1 copy.34
  115.3 0.1 eq.40
  115.5 0.2 fusion
  115.7 0.1 convert_element_type.30
  115.8 0.1 copy.35
  115.9 0.7 fusion.3.pick_ref
  116.6 4.6 %shard_map.133 = (bf16[128,4096]{1,0:T(8,128)(2,1)}, bf16[256,4096]{1,0:T(8,128)(2,1)}, bf16[128,4096]{1,0:T(8,128)(2,1)}) custom-call(bf16[4,128,1024]{2,1,0:T(8,128)(2,1)} %shard_map.132.parts_ref, bf16[128,4096]{1,0:T(8,128)(2,1)} %bitcast.55, f32[1,4096]{1,0:T(1,128)} %bitcast.59, f32[1,4096]{1,0:T(1,128)} %bitcast.60, bf16[384,128]{1,0:T(8,128)(2,1)} %fusion.3.pick_ref), custom_call_target="tpu_custom_call" | custom-call | tf_op jit(solution)/shard_map/pallas_call | solution.py:217
  121.2 2.2 reshape.49.refs_1_
  123.5 79.8 %shard_map.134 = (bf16[32,8,4096]{2,1,0:T(8,128)(2,1)}, bf16[32,4,4096]{2,1,0:T(4,128)(2,1)}) custom-call(bf16[32,8,4096]{2,1,0:T(8,128)(2,1)} %bitcast.52, bf16[32,4,4096]{2,1,0:T(4,128)(2,1)} %reshape.49.refs_1_), custom_call_target="tpu_custom_call" | custom-call | bytes 62914560 | tf_op jit(solution)/shard_map/pallas_call | solution.py:93
  203.2 2.1 reshape.51.refs_1_
  205.4 11.8 %shard_map.135 = (bf16[256,4096]{1,0:T(8,128)(2,1)}, bf16[128,4096]{1,0:T(8,128)(2,1)}) custom-call(bf16[256,4096]{1,0:T(8,128)(2,1)} %bitcast.47, bf16[128,4096]{1,0:T(8,128)(2,1)} %reshape.51.refs_1_, bf16[4096,512]{1,0:T(8,128)(2,1)} %bitcast.44, bf16[4096,512]{1,0:T(8,128)(2,1)} %bitcast.45, bf16[512,4096]{1,0:T(8,128)(2,1)} %bitcast.46), custom_call_target="tpu_custom_call" | custom-call | tf_op jit(solution)/shard_map/pallas_call | solution.py:240
  217.1 2.2 reshape.53.refs_1_
  219.4 0.0 copy-start.2
  219.4 79.4 %shard_map.136 = (bf16[32,8,4096]{2,1,0:T(8,128)(2,1)}, bf16[32,4,4096]{2,1,0:T(4,128)(2,1)}) custom-call(bf16[32,8,4096]{2,1,0:T(8,128)(2,1)} %bitcast.53, bf16[32,4,4096]{2,1,0:T(4,128)(2,1)} %reshape.53.refs_1_), custom_call_target="tpu_custom_call" | custom-call | bytes 62914560 | tf_op jit(solution)/shard_map/pallas_call | solution.py:93
  298.8 2.2 reshape.55.refs_1_
  301.0 0.0 copy-done.2
  301.0 0.8 subtract_convert_fusion
  301.8 5.1 %shard_map.137 = bf16[128,4096]{1,0:T(8,128)(2,1)} custom-call(bf16[256,4096]{1,0:T(8,128)(2,1)} %bitcast.54, bf16[128,4096]{1,0:T(8,128)(2,1)} %reshape.55.refs_1_, bf16[128,384]{1,0:T(8,128)(2,1)} %get-tuple-element.30.refs_2_, bf16[128,384]{1,0:T(8,128)(2,1)} %get-tuple-element.29.refs_3_, bf16[128,4096]{1,0:T(8,128)(2,1)} %get-tuple-element.28.refs_4_, ...), custom_call_target="tpu_custom_call" | custom-call | tf_op jit(solution)/shard_map/pallas_call | solution.py:266
  (4 shorter events, 0.0 us)
Async XLA Ops:
  0.0 4.0 %copy-start = (bf16[1,128,16,128]{3,2,1,0:T(8,128)(2,1)S(1)}, bf16[1,128,16,128]{3,2,1,0:T(8,128)(2,1)}, u32[]{:S(2)}) copy-start(bf16[1,128,16,128]{3,2,1,0:T(8,128)(2,1)} %param.15) | copy-start | bytes 1572868
  101.1 14.1 %copy-start.1 = (s32[1,128,2]{1,2,0:T(2,128)S(1)}, s32[1,128,2]{1,2,0:T(2,128)}, u32[]{:S(2)}) copy-start(s32[1,128,2]{1,2,0:T(2,128)} %param.23) | copy-start | bytes 3076
  219.4 81.6 %copy-start.2 = (f32[1,128,2]{1,2,0:T(2,128)S(1)}, f32[1,128,2]{1,2,0:T(2,128)}, u32[]{:S(2)}) copy-start(f32[1,128,2]{1,2,0:T(2,128)} %param.24) | copy-start | bytes 3076
where the time goes:
time: 307 us
  Pallas kernels  288 us (94%)
  local copies, waits for them, and re-layouts  17.1 us (6%)
    pallas_call x6, Pallas kernels, exchange(): pl.pallas_call(functools.partial(exchange_kernel, axes, sizes, n, count),...  252 us
    pallas_call x1, Pallas kernels, serve(): pl.pallas_call(functools.partial(expert_kernel, len(arrays)), out_shape=[...  11.8 us
    pallas_call x1, Pallas kernels, attend(): pl.pallas_call(functools.partial(attend_kernel, block), grid=(heads,), ou...  8.55 us
    pallas_call x1, Pallas kernels, project(): pl.pallas_call(project_kernel, out_shape=jax.ShapeDtypeStruct((parts, row...  6.14 us

commit v1 on v0

--- a/solution.py
+++ b/solution.py
@@ -108,119 +108,343 @@
     )(*arrays)
 
 
-def attend_kernel(block, q_ref, k_ref, v_ref, out_ref):
-    sources, _, rows, width = q_ref.shape
-    length = sources * rows
+CHUNKS = 8
+RELAYED = 3
+DIRECT = 2
+
+
+def front_kernel(sp, dp, groups, *refs):
+    q_ref, k_ref, v_ref, weight_ref, resid_ref, mixer_ref, expert_ref, pick_ref = refs[:8]
+    stream_ref = refs[8]
+    sent_refs = refs[9 : 9 + groups]
+    (
+        stage, arrived, out_heads, in_heads, flat, full, projected, tokens,
+        q_send, q_recv, a_send, a_recv, near_sem, far_send, far_recv, relay_send, relay_recv,
+        twin_send, twin_recv, last_send, last_recv, local_sem,
+    ) = refs[9 + groups :]
+    rows, heads, width = q_ref.shape
+    local_heads = heads // sp
+    depth, columns = weight_ref.shape
+    me, mate = lax.axis_index("sp"), lax.axis_index("dp")
+    parity, core = lax.rem(me, 2), lax.rem(mate, 2)
+    side, twin = me + 1 - 2 * parity, mate + 1 - 2 * core
+    ys = dp // 2
+    own_y = lax.div(mate, 2)
+
+    def signal(device):
+        pl.semaphore_signal(barrier, inc=1, device_id=device, device_id_type=MESH)
+
+    barrier = pltpu.get_barrier_semaphore()
+
+    def greet_sp(k, carry):
+        signal({"sp": lax.rem(me + k, sp)})
+        return carry
+
+    lax.fori_loop(1, sp, greet_sp, 0)
+    signal({"dp": twin})
+    for d in range(1, ys):
+        signal({"dp": lax.rem(own_y + d, ys) * 2 + core})
+    load = pltpu.make_async_copy(weight_ref, full.at[mate], local_sem.at[0])
+    load.start()
+    stage[0] = jnp.transpose(q_ref[...], (1, 0, 2))
+    stage[1] = jnp.transpose(k_ref[...], (1, 0, 2))
+    pl.semaphore_wait(barrier, sp - 1 + 1 + ys - 1)
+
+    def head_copy(t, h, k):
+        target = lax.rem(me + k, sp)
+        return pltpu.make_async_remote_copy(
+            src_ref=stage.at[t, target * local_heads + h],
+            dst_ref=arrived.at[t, me, h],
+            send_sem=q_send.at[t, h, k],
+            recv_sem=q_recv.at[t, h, k],
+            device_id={"sp": target},
+            device_id_type=MESH,
+        )
+
+    def send_heads(t, h):
+        def push(i, carry):
+            k = sp // 2 + (1 - 2 * lax.rem(i, 2)) * lax.div(i + 1, 2)
+            head_copy(t, h, k).start()
+            return carry
+
+        lax.fori_loop(0, sp - 1, push, 0)
+
+    def finish(make, low, high):
+        def body(k, carry):
+            make(k).wait()
+            return carry
+
+        lax.fori_loop(low, high, body, 0)
+
+    span = depth // CHUNKS
+
+    def chunk(owner_parity, j):
+        if j < RELAYED:
+            return pl.ds(pl.multiple_of((owner_parity * (RELAYED + DIRECT) + j) * span, span), span)
+        return pl.ds(j * span, span)
+
+    def shift(src, dst, sends, recvs, index, device):
+        return pltpu.make_async_remote_copy(
+            src_ref=src, dst_ref=dst, send_sem=sends.at[index], recv_sem=recvs.at[index],
+            device_id=device, device_id_type=MESH,
+        )
+
+    def far(d, j):
+        where = chunk(parity, j)
+        return shift(
+            weight_ref.at[where], full.at[mate, where], far_send, far_recv, (d - 1, j),
+            {"dp": lax.rem(own_y + d, ys) * 2 + core},
+        )
+
+    def relay(d, j):
+        origin = lax.rem(own_y + ys - d, ys) * 2 + core
+        where = chunk(parity, j)
+        block = full.at[origin, where]
+        return shift(block, block, relay_send, relay_recv, (d - 1, j), {"sp": side})
+
+    def to_twin(d, j):
+        origin = lax.rem(own_y + ys - d, ys) * 2 + core
+        block = full.at[origin, chunk(parity, j)]
+        return shift(block, block, twin_send, twin_recv, (d - 1, j), {"dp": twin})
+
+    def to_twin_last(d, j):
+        origin = lax.rem(own_y + ys - d, ys) * 2 + core
+        block = full.at[origin, chunk(1 - parity, j)]
+        return shift(block, block, last_send, last_recv, (d - 1, j), {"dp": twin})
+
+    near = pltpu.make_async_remote_copy(
+        src_ref=weight_ref, dst_ref=full.at[mate], send_sem=near_sem.at[0], recv_sem=near_sem.at[1],
+        device_id={"dp": twin}, device_id_type=MESH,
+    )
+    for d in range(1, ys):
+        far(d, 0).start()
+    for h in range(local_heads):
+        send_heads(0, h)
+    for d in range(1, ys):
+        for j in range(1, RELAYED + DIRECT):
+            far(d, j).start()
+    near.start()
+    stage[2] = jnp.transpose(v_ref[...], (1, 0, 2))
+    own = [
+        pltpu.make_async_copy(
+            stage.at[t, pl.ds(me * local_heads, local_heads)], arrived.at[t, me], local_sem.at[1 + t]
+        )
+        for t in range(3)
+    ]
+    for h in range(local_heads):
+        send_heads(1, h)
+    for copy in own[:2]:
+        copy.start()
+    for h in range(local_heads):
+        send_heads(2, h)
+    own[2].start()
+
+    block = rows * max(1, min(sp, 256 // rows))
+    per = block // rows
+    length = sp * rows
     scale = width ** (-0.5)
     tri_row = lax.broadcasted_iota(jnp.int32, (block, block), 0)
     tri_col = lax.broadcasted_iota(jnp.int32, (block, block), 1)
     suffix_ones = (tri_row >= tri_col).astype(jnp.bfloat16)
     is_past = tri_col < tri_row
-    per = block // rows
-
-    def piece(ref, index):
-        return ref[index * per : (index + 1) * per, 0].reshape(block, width)
-
-    for q_block in range(length // block):
-        query = piece(q_ref, q_block)
-        total = jnp.zeros((block, width), jnp.float32)
-        later = jnp.zeros((block, 1), jnp.float32)
-        for k_block in range(q_block, -1, -1):
-            scores = (
-                lax.dot_general(
-                    query,
-                    piece(k_ref, k_block),
-                    (((1,), (1,)), ((), ())),
-                    preferred_element_type=jnp.float32,
+
+    def answer(h, target):
+        return pltpu.make_async_remote_copy(
+            src_ref=out_heads.at[h, target],
+            dst_ref=in_heads.at[me, h],
+            send_sem=a_send.at[h, target],
+            recv_sem=a_recv.at[h, me],
+            device_id={"sp": target},
+            device_id_type=MESH,
+        )
+
+    def expect(h, source):
+        return pltpu.make_async_remote_copy(
+            src_ref=out_heads.at[h, source],
+            dst_ref=in_heads.at[source, h],
+            send_sem=a_send.at[h, source],
+            recv_sem=a_recv.at[h, source],
+            device_id={"sp": source},
+            device_id_type=MESH,
+        )
+
+    def attend_head(h):
+        def piece(t, index):
+            return arrived[t, index * per : (index + 1) * per, h].reshape(block, width)
+
+        for q_block in range(length // block):
+            query = piece(0, q_block)
+            total = jnp.zeros((block, width), jnp.float32)
+            later = jnp.zeros((block, 1), jnp.float32)
+            for k_block in range(q_block, -1, -1):
+                scores = (
+                    lax.dot_general(
+                        query, piece(1, k_block), (((1,), (1,)), ((), ())),
+                        preferred_element_type=jnp.float32,
+                    )
+                    * scale
                 )
-                * scale
+                soft = jnp.maximum(scores, 0.0) + jnp.log(1.0 + jnp.exp(-jnp.abs(scores)))
+                if k_block == q_block:
+                    soft = jnp.where(is_past, soft, 0.0)
+                high = soft.astype(jnp.bfloat16)
+                low = (soft - high.astype(jnp.float32)).astype(jnp.bfloat16)
+                suffix = jnp.dot(high, suffix_ones, preferred_element_type=jnp.float32) + jnp.dot(
+                    low, suffix_ones, preferred_element_type=jnp.float32
+                )
+                weights = jnp.exp(scores - suffix - later)
+                if k_block == q_block:
+                    weights = jnp.where(is_past, weights, 0.0)
+                total = total + jnp.dot(
+                    weights.astype(jnp.bfloat16), piece(2, k_block), preferred_element_type=jnp.float32
+                )
+                if k_block > 0:
+                    later = later + suffix[:, :1]
+            out_heads[h, q_block * per : (q_block + 1) * per] = total.astype(jnp.bfloat16).reshape(
+                per, rows, width
             )
-            soft = jnp.maximum(scores, 0.0) + jnp.log(1.0 + jnp.exp(-jnp.abs(scores)))
-            if k_block == q_block:
-                soft = jnp.where(is_past, soft, 0.0)
-            high = soft.astype(jnp.bfloat16)
-            low = (soft - high.astype(jnp.float32)).astype(jnp.bfloat16)
-            suffix = jnp.dot(high, suffix_ones, preferred_element_type=jnp.float32) + jnp.dot(
-                low, suffix_ones, preferred_element_type=jnp.float32
+
+    def send_answers(h):
+        def push(k, carry):
+            answer(h, lax.rem(me + k, sp)).start()
+            return carry
+
+        lax.fori_loop(1, sp, push, 0)
+        pltpu.make_async_copy(out_heads.at[h, me], in_heads.at[me, h], local_sem.at[4 + h]).start()
+
+    def pass_on(j):
+        for d in range(1, ys):
+            far(d, j).wait_recv()
+            if j < RELAYED:
+                relay(d, j).start()
+            to_twin(d, j).start()
+
+    def pass_last(j):
+        for d in range(1, ys):
+            pltpu.make_async_remote_copy(
+                src_ref=full.at[0, chunk(1 - parity, j)],
+                dst_ref=full.at[0, chunk(1 - parity, j)],
+                send_sem=relay_send.at[d - 1, j], recv_sem=relay_recv.at[d - 1, j],
+                device_id={"sp": side}, device_id_type=MESH,
+            ).wait_recv()
+            to_twin_last(d, j).start()
+
+    pass_on(0)
+    for h in range(local_heads):
+        if h == 0:
+            for copy in own:
+                copy.wait()
+        for t in range(3):
+            finish(lambda k: head_copy(t, h, k), 1, sp)
+        attend_head(h)
+        send_answers(h)
+        if h == 0:
+            pass_on(1)
+    pass_last(0)
+    pass_on(2)
+    pass_last(1)
+    for j in range(RELAYED, RELAYED + DIRECT):
+        pass_on(j)
+        if j == RELAYED:
+            pass_last(2)
+
+    for h in range(local_heads):
+        finish(lambda k: expect(h, lax.rem(me + k, sp)), 1, sp)
+        pltpu.make_async_copy(out_heads.at[h, me], in_heads.at[me, h], local_sem.at[4 + h]).wait()
+    for source in range(sp):
+        for h in range(local_heads):
+            place = (source * local_heads + h) * width
+            flat[:, place : place + width] = in_heads[source, h]
+    load.wait()
+    near.wait()
+    for d in range(1, ys):
+        for j in range(RELAYED + DIRECT):
+            far(d, j).wait_send()
+            to_twin(d, j).wait()
+            if j < RELAYED:
+                relay(d, j).wait_send()
+                to_twin_last(d, j).wait()
+
+    tile = min(columns, 512)
+    many = columns // tile
+
+    @pl.loop(0, dp * many)
+    def _(i):
+        inner = pl.ds(pl.multiple_of(lax.rem(i, many) * tile, tile), tile)
+        outer = pl.ds(pl.multiple_of(i * tile, tile), tile)
+        projected[:, outer] = jnp.dot(
+            flat[...], full[lax.div(i, many), :, inner], preferred_element_type=jnp.float32
+        )
+
+    @pl.loop(0, rows // 16)
+    def _(i):
+        part = pl.ds(pl.multiple_of(i * 16, 16), 16)
+        stream = (
+            resid_ref[part].astype(jnp.float32) + normed_token_rows(projected[part], mixer_ref[...])
+        ).astype(jnp.bfloat16)
+        stream_ref[part] = stream
+        tokens[part] = normed_token_rows(stream.astype(jnp.float32), expert_ref[...]).astype(jnp.bfloat16)
+
+    features = projected.shape[1]
+
+    @pl.loop(0, features // 512)
+    def _(i):
+        part = pl.ds(pl.multiple_of(i * 512, 512), 512)
+        row = 0
+        for ref in sent_refs:
+            many_rows = ref.shape[0] * ref.shape[1]
+            ref[:, :, part] = (
+                jnp.dot(pick_ref[row : row + many_rows], tokens[:, part], preferred_element_type=jnp.float32)
+                .astype(jnp.bfloat16)
+                .reshape(ref.shape[0], ref.shape[1], 512)
             )
-            weights = jnp.exp(scores - suffix - later)
-            if k_block == q_block:
-                weights = jnp.where(is_past, weights, 0.0)
-            total = total + jnp.dot(
-                weights.astype(jnp.bfloat16),
-                piece(v_ref, k_block),
-                preferred_element_type=jnp.float32,
-            )
-            if k_block > 0:
-                later = later + suffix[:, :1]
-        out_ref[q_block * per : (q_block + 1) * per, 0] = total.astype(jnp.bfloat16).reshape(
-            per, rows, width
-        )
-
-
-def attend(query, key, value):
-    sources, heads, rows, width = query.shape
-    block = rows * max(1, min(sources, 256 // rows))
-    spec = pl.BlockSpec((sources, 1, rows, width), lambda h: (0, h, 0, 0))
+            row += many_rows
+
+
+def front(query, key, value, weight, residual, mixer_gain, expert_gain, pick, experts, groups):
+    sp, dp = lax.axis_size("sp"), lax.axis_size("dp")
+    rows, heads, width = query.shape
+    depth, columns = weight.shape
+    features = residual.shape[1]
+    local_heads = heads // sp
+    ys = max(dp // 2 - 1, 1)
+    whole = pl.BlockSpec(memory_space=pltpu.VMEM)
+    dma = pltpu.SemaphoreType.DMA
+    bf16 = jnp.bfloat16
     return pl.pallas_call(
-        functools.partial(attend_kernel, block),
-        grid=(heads,),
-        out_shape=jax.ShapeDtypeStruct(query.shape, jnp.bfloat16),
-        in_specs=[spec] * 3,
-        out_specs=spec,
-        compiler_params=pltpu.CompilerParams(vmem_limit_bytes=VMEM_LIMIT),
-        cost_estimate=pl.CostEstimate(
-            flops=6 * heads * (sources * rows) ** 2 * width, bytes_accessed=8 * query.size, transcendentals=0
+        functools.partial(front_kernel, sp, dp, len(groups)),
+        out_shape=[jax.ShapeDtypeStruct((rows, features), bf16)]
+        + [jax.ShapeDtypeStruct((experts, g, features), bf16) for g in groups],
+        in_specs=[whole] * 3 + [pl.BlockSpec(memory_space=pl.ANY)] + [whole] * 4,
+        out_specs=[whole] * (1 + len(groups)),
+        scratch_shapes=[
+            pltpu.VMEM((3, heads, rows, width), bf16),
+            pltpu.VMEM((3, sp, local_heads, rows, width), bf16),
+            pltpu.VMEM((local_heads, sp, rows, width), bf16),
+            pltpu.VMEM((sp, local_heads, rows, width), bf16),
+            pltpu.VMEM((rows, depth), bf16),
+            pltpu.VMEM((dp, depth, columns), bf16),
+            pltpu.VMEM((rows, features), jnp.float32),
+            pltpu.VMEM((rows, features), bf16),
+            dma((3, local_heads, sp)),
+            dma((3, local_heads, sp)),
+            dma((local_heads, sp)),
+            dma((local_heads, sp)),
+            dma((2,)),
+            dma((ys, RELAYED + DIRECT)),
+            dma((ys, RELAYED + DIRECT)),
+            dma((ys, RELAYED)),
+            dma((ys, RELAYED)),
+            dma((ys, RELAYED + DIRECT)),
+            dma((ys, RELAYED + DIRECT)),
+            dma((ys, RELAYED)),
+            dma((ys, RELAYED)),
+            dma((4 + local_heads,)),
+        ],
+        compiler_params=pltpu.CompilerParams(
+            collective_id=0, has_side_effects=True, vmem_limit_bytes=VMEM_LIMIT
         ),
-    )(query, key, value)
-
-
-def project_kernel(attn_ref, weight_ref, out_ref):
-    for part in range(attn_ref.shape[0]):
-        flat = jnp.concatenate([attn_ref[part, h] for h in range(attn_ref.shape[1])], axis=1)
-        out_ref[part] = jnp.dot(
-            flat, weight_ref[...], preferred_element_type=jnp.float32
-        ).astype(jnp.bfloat16)
-
-
-def project(attn, weight):
-    parts, _, rows, _ = attn.shape
-    return pl.pallas_call(
-        project_kernel,
-        out_shape=jax.ShapeDtypeStruct((parts, rows, weight.shape[1]), jnp.bfloat16),
-        in_specs=[pl.BlockSpec(memory_space=pltpu.VMEM)] * 2,
-        out_specs=pl.BlockSpec(memory_space=pltpu.VMEM),
-        compiler_params=pltpu.CompilerParams(vmem_limit_bytes=VMEM_LIMIT),
-    )(attn, weight)
-
-
-def mix_kernel(parts_ref, resid_ref, mixer_ref, expert_ref, pick_ref, stream_ref, *sent_refs):
-    projected = jnp.concatenate(
-        [parts_ref[part].astype(jnp.float32) for part in range(parts_ref.shape[0])], axis=1
-    )
-    stream = (
-        resid_ref[...].astype(jnp.float32) + normed_token_rows(projected, mixer_ref[...])
-    ).astype(jnp.bfloat16)
-    stream_ref[...] = stream
-    tokens = normed_token_rows(stream.astype(jnp.float32), expert_ref[...]).astype(jnp.bfloat16)
-    row = 0
-    for ref in sent_refs:
-        many = ref.shape[0]
-        ref[...] = jnp.dot(
-            pick_ref[row : row + many], tokens, preferred_element_type=jnp.float32
-        ).astype(jnp.bfloat16)
-        row += many
-
-
-def mix(parts, residual, mixer_gain, expert_gain, pick, splits):
-    rows, features = residual.shape
-    return pl.pallas_call(
-        mix_kernel,
-        out_shape=[jax.ShapeDtypeStruct((many, features), jnp.bfloat16) for many in [rows] + splits],
-        in_specs=[pl.BlockSpec(memory_space=pltpu.VMEM)] * 5,
-        out_specs=[pl.BlockSpec(memory_space=pltpu.VMEM)] * (1 + len(splits)),
-        compiler_params=pltpu.CompilerParams(vmem_limit_bytes=VMEM_LIMIT),
-    )(parts, residual, mixer_gain[None], expert_gain[None], pick)
+    )(query, key, value, weight, residual, mixer_gain[None], expert_gain[None], pick)
 
 
 def expert_kernel(count, *refs):
@@ -291,18 +515,7 @@
     _, local_rows, heads, width = queries.shape
     features = residual.shape[2]
 
-    def by_head(tensor):
-        return jnp.transpose(tensor[0], (1, 0, 2)).reshape(sp, heads // sp, local_rows, width)
-
-    head_parts = exchange([by_head(queries), by_head(key_rows), by_head(values)], ("sp",), 0)
-    attended = attend(*head_parts)
-    (token_parts,) = exchange([attended], ("sp",), 1)
-
     dp = lax.axis_size("dp")
-    token_heads = token_parts.reshape(heads, local_rows, width)
-    (group_heads,) = exchange([jnp.broadcast_to(token_heads[None], (dp,) + token_heads.shape)], ("dp",), 4)
-    (projected_parts,) = exchange([project(group_heads, out_weight)], ("dp",), 5)
-
     experts = sp * dp
     top_count = routes.shape[2]
     capacity = max(2, 3 * local_rows // experts)
@@ -332,13 +545,8 @@
     share_high = share.astype(jnp.bfloat16)
     share_low = (share - share_high.astype(jnp.float32)).astype(jnp.bfloat16)
 
-    stream, *outgoing = mix(
-        projected_parts,
-        residual[0],
-        mixer_gain,
-        expert_gain,
-        pick,
-        splits,
+    stream, *outgoing = front(
+        queries[0], key_rows[0], values[0], out_weight, residual[0], mixer_gain, expert_gain, pick, experts, groups
     )
 
     def blocks(arrays):
@@ -347,7 +555,7 @@
     def flat(arrays):
         return [a.reshape(-1, features) for a in arrays]
 
-    arrived = exchange(blocks(outgoing), ("sp", "dp"), 2)
+    arrived = exchange(outgoing, ("sp", "dp"), 2)
     results = serve(flat(arrived), gate_weight[0], up_weight[0], expert_down_matrix[0])
     returned = exchange(blocks(results), ("sp", "dp"), 3)
     output = combine(flat(returned), share_high, share_low, stream, output_gain)

time: 307 us -> 269 us (0.88)
  Pallas kernels: 288 us -> 259 us
  local copies, waits for them, and re-layouts: 17.1 us -> 7.67 us
    pallas_call x6 -> x2, Pallas kernels: 252 us -> 160 us  [exchange(): pl.pallas_call(functools.partial(exchange_kernel, axes, sizes, n, count),...]
    pallas_call x3 -> x1, Pallas kernels: 19.3 us -> 81.8 us  [front(): pl.pallas_call(functools.partial(front_kernel, sp, dp, len(groups)), out_...]
    transpose x3 -> x0, local copies, waits for them, and re-layouts: 4.95 us -> none  [by_head(): jnp.transpose(tensor[0], (1, 0, 2))]
where the time goes in v1:
time: 269 us
  Pallas kernels  259 us (96%)
  local copies, waits for them, and re-layouts  7.67 us (3%)
    pallas_call x2, Pallas kernels, exchange(): pl.pallas_call(functools.partial(exchange_kernel, axes, sizes, n, count),...  160 us
    pallas_call x1, Pallas kernels, front(): pl.pallas_call(functools.partial(front_kernel, sp, dp, len(groups)), out_...  81.8 us
    pallas_call x1, Pallas kernels, serve(): pl.pallas_call(functools.partial(expert_kernel, len(arrays)), out_shape=[...  11.8 us

profile of v1, /device:TPU:16, one launch (start us, length us, event | category | flops | bytes accessed | tf_op | source)
XLA Modules:
  0.0 269.2 jit_solution(12480265704463706929)
XLA Ops:
  0.0 0.8 copy.22
  0.8 0.1 eq.40
  0.9 0.2 fusion
  1.1 0.1 convert_element_type.30
  1.3 0.1 copy.23
  1.3 0.7 and_select_fusion.1
  2.1 0.7 fusion.3.refs_7_
  2.7 81.8 %shard_map.127 = (bf16[128,4096]{1,0:T(8,128)(2,1)}, bf16[32,8,4096]{2,1,0:T(8,128)(2,1)}, bf16[32,4,4096]{2,1,0:T(4,128)(2,1)}) custom-call(bf16[128,16,128]{2,1,0:T(8,128)(2,1)} %bitcast.40, bf16[128,16,128]{2,1,0:T(8,128)(2,1)} %bitcast.41, bf16[128,16,128]{2,1,0:T(8,128)(2,1)} %bitcast.42, bf16[2048,1024]{1,0:T(8,128)(2,1)} %refs_3_.1, ...), custom_call_target="tpu_custom_call" | custom-call | tf_op jit(solution)/shard_map/pallas_call | solution.py:414
  84.6 80.9 %shard_map.128 = (bf16[32,8,4096]{2,1,0:T(8,128)(2,1)}, bf16[32,4,4096]{2,1,0:T(4,128)(2,1)}) custom-call(bf16[32,8,4096]{2,1,0:T(8,128)(2,1)} %get-tuple-element.14.refs_0_, bf16[32,4,4096]{2,1,0:T(4,128)(2,1)} %get-tuple-element.15.refs_1_), custom_call_target="tpu_custom_call" | custom-call | bytes 62914560 | tf_op jit(solution)/shard_map/pallas_call | solution.py:93
  165.5 2.1 reshape.30.refs_1_
  167.7 11.8 %shard_map.129 = (bf16[256,4096]{1,0:T(8,128)(2,1)}, bf16[128,4096]{1,0:T(8,128)(2,1)}) custom-call(bf16[256,4096]{1,0:T(8,128)(2,1)} %bitcast.36, bf16[128,4096]{1,0:T(8,128)(2,1)} %reshape.30.refs_1_, bf16[4096,512]{1,0:T(8,128)(2,1)} %bitcast.33, bf16[4096,512]{1,0:T(8,128)(2,1)} %bitcast.34, bf16[512,4096]{1,0:T(8,128)(2,1)} %bitcast.35), custom_call_target="tpu_custom_call" | custom-call | tf_op jit(solution)/shard_map/pallas_call | solution.py:464
  179.5 0.0 copy-start
  179.5 2.2 reshape.32.refs_1_
  181.7 79.4 %shard_map.130 = (bf16[32,8,4096]{2,1,0:T(8,128)(2,1)}, bf16[32,4,4096]{2,1,0:T(4,128)(2,1)}) custom-call(bf16[32,8,4096]{2,1,0:T(8,128)(2,1)} %bitcast.37, bf16[32,4,4096]{2,1,0:T(4,128)(2,1)} %reshape.32.refs_1_), custom_call_target="tpu_custom_call" | custom-call | bytes 62914560 | tf_op jit(solution)/shard_map/pallas_call | solution.py:93
  261.1 2.2 reshape.34.refs_1_
  263.3 0.0 copy-done
  263.3 0.8 subtract_convert_fusion
  264.1 5.1 %shard_map.131 = bf16[128,4096]{1,0:T(8,128)(2,1)} custom-call(bf16[256,4096]{1,0:T(8,128)(2,1)} %bitcast.38, bf16[128,4096]{1,0:T(8,128)(2,1)} %reshape.34.refs_1_, bf16[128,384]{1,0:T(8,128)(2,1)} %get-tuple-element.24.refs_2_, bf16[128,384]{1,0:T(8,128)(2,1)} %get-tuple-element.23.refs_3_, bf16[128,4096]{1,0:T(8,128)(2,1)} %get-tuple-element.22.refs_4_, ...), custom_call_target="tpu_custom_call" | custom-call | tf_op jit(solution)/shard_map/pallas_call | solution.py:490
  (3 shorter events, 0.0 us)
Async XLA Ops:
  179.5 83.8 %copy-start = (f32[1,128,2]{1,2,0:T(2,128)S(1)}, f32[1,128,2]{1,2,0:T(2,128)}, u32[]{:S(2)}) copy-start(f32[1,128,2]{1,2,0:T(2,128)} %param.24) | copy-start | bytes 3076

commit v2 on v1

--- a/solution.py
+++ b/solution.py
@@ -20,92 +20,6 @@
     if len(axes) == 1:
         return {axes[0]: flat}
     return {axes[0]: lax.div(flat, sizes[1]), axes[1]: lax.rem(flat, sizes[1])}
-
-
-def exchange_kernel(axes, sizes, n, count, *refs):
-    ins, outs = refs[:count], refs[count : 2 * count]
-    stages = refs[2 * count : 3 * count]
-    send_sem, recv_sem, local_sem = refs[3 * count :]
-    me = lax.axis_index(axes[0])
-    if len(axes) == 2:
-        me = me * sizes[1] + lax.axis_index(axes[1])
-
-    barrier = pltpu.get_barrier_semaphore()
-
-    def greet(k, carry):
-        pl.semaphore_signal(
-            barrier, inc=1, device_id=peer_id(axes, sizes, lax.rem(me + k, n)), device_id_type=MESH
-        )
-        return carry
-
-    lax.fori_loop(1, n, greet, 0)
-    loads = [
-        pltpu.make_async_copy(ins[a].at[me], stages[a], local_sem.at[a]) for a in range(count)
-    ]
-    for load in loads:
-        load.start()
-    pl.semaphore_wait(barrier, n - 1)
-
-    def copies(k):
-        target = lax.rem(me + k, n)
-        return [
-            pltpu.make_async_remote_copy(
-                src_ref=ins[a].at[target],
-                dst_ref=outs[a].at[me],
-                send_sem=send_sem.at[a, k],
-                recv_sem=recv_sem.at[a, k],
-                device_id=peer_id(axes, sizes, target),
-                device_id_type=MESH,
-            )
-            for a in range(count)
-        ]
-
-    def push(i, carry):
-        k = n // 2 + (1 - 2 * lax.rem(i, 2)) * lax.div(i + 1, 2)
-        for copy in copies(k):
-            copy.start()
-        return carry
-
-    lax.fori_loop(0, n - 1, push, 0)
-    stores = [
-        pltpu.make_async_copy(stages[a], outs[a].at[me], local_sem.at[a]) for a in range(count)
-    ]
-    for load in loads:
-        load.wait()
-    for store in stores:
-        store.start()
-    for store in stores:
-        store.wait()
-
-    def finish(k, carry):
-        for copy in copies(k):
-            copy.wait()
-        return carry
-
-    lax.fori_loop(1, n, finish, 0)
-
-
-def exchange(arrays, axes, collective_id):
-    sizes = [lax.axis_size(a) for a in axes]
-    n = arrays[0].shape[0]
-    count = len(arrays)
-    moved = sum(a.size * 2 for a in arrays)
-    return pl.pallas_call(
-        functools.partial(exchange_kernel, axes, sizes, n, count),
-        out_shape=[jax.ShapeDtypeStruct(a.shape, a.dtype) for a in arrays],
-        in_specs=[pl.BlockSpec(memory_space=pl.ANY)] * count,
-        out_specs=[pl.BlockSpec(memory_space=pl.ANY)] * count,
-        scratch_shapes=[pltpu.VMEM(a.shape[1:], a.dtype) for a in arrays]
-        + [
-            pltpu.SemaphoreType.DMA((count, n)),
-            pltpu.SemaphoreType.DMA((count, n)),
-            pltpu.SemaphoreType.DMA((count,)),
-        ],
-        compiler_params=pltpu.CompilerParams(
-            collective_id=collective_id, has_side_effects=True, vmem_limit_bytes=VMEM_LIMIT
-        ),
-        cost_estimate=pl.CostEstimate(flops=0, bytes_accessed=moved * 20, transcendentals=0),
-    )(*arrays)
 
 
 CHUNKS = 8
@@ -447,53 +361,144 @@
     )(query, key, value, weight, residual, mixer_gain[None], expert_gain[None], pick)
 
 
-def expert_kernel(count, *refs):
-    ins, (gate_ref, up_ref, down_ref) = refs[:count], refs[count : count + 3]
-    outs = refs[count + 3 :]
+def back_kernel(axes, sizes, n, count, *refs):
+    sent = refs[:count]
+    gate_hbm, up_hbm, down_hbm, high_ref, low_ref, stream_ref, gain_ref, out_ref = refs[count : count + 8]
+    rest = refs[count + 8 :]
+    arrived, results, returned = rest[:count], rest[count : 2 * count], rest[2 * count : 3 * count]
+    (
+        gate_ref, up_ref, down_ref, combined,
+        send_sem, recv_sem, back_send, back_recv, local_sem, weight_sem,
+    ) = rest[3 * count :]
+    me = lax.axis_index(axes[0]) * sizes[1] + lax.axis_index(axes[1])
+    features = stream_ref.shape[1]
+    tile = min(features, 512)
+
+    barrier = pltpu.get_barrier_semaphore()
+
+    def greet(k, carry):
+        pl.semaphore_signal(
+            barrier, inc=1, device_id=peer_id(axes, sizes, lax.rem(me + k, n)), device_id_type=MESH
+        )
+        return carry
+
+    lax.fori_loop(1, n, greet, 0)
+    loads = [pltpu.make_async_copy(sent[a].at[me], arrived[a].at[me], local_sem.at[a]) for a in range(count)]
+    keeps = [
+        pltpu.make_async_copy(results[a].at[me], returned[a].at[me], local_sem.at[count + a])
+        for a in range(count)
+    ]
+    fetches = [
+        pltpu.make_async_copy(src, dst, weight_sem.at[i])
+        for i, (src, dst) in enumerate(((gate_hbm, gate_ref), (up_hbm, up_ref), (down_hbm, down_ref)))
+    ]
+    for copy in loads + fetches:
+        copy.start()
+    pl.semaphore_wait(barrier, n - 1)
+
+    def move(sources, targets, sends, recvs, a, k):
+        target = lax.rem(me + k, n)
+        return pltpu.make_async_remote_copy(
+            src_ref=sources[a].at[target],
+            dst_ref=targets[a].at[me],
+            send_sem=sends.at[a, k],
+            recv_sem=recvs.at[a, k],
+            device_id=peer_id(axes, sizes, target),
+            device_id_type=MESH,
+        )
+
+    def outward(a, k):
+        return move(sent, arrived, send_sem, recv_sem, a, k)
+
+    def homeward(a, k):
+        return move(results, returned, back_send, back_recv, a, k)
+
+    def start_all(make, a):
+        def push(i, carry):
+            k = n // 2 + (1 - 2 * lax.rem(i, 2)) * lax.div(i + 1, 2)
+            make(a, k).start()
+            return carry
+
+        lax.fori_loop(0, n - 1, push, 0)
+
+    def wait_all(make, a):
+        def body(k, carry):
+            make(a, k).wait()
+            return carry
+
+        lax.fori_loop(1, n, body, 0)
+
     for a in range(count):
-        rows = ins[a][...]
+        start_all(outward, a)
+    for a in range(count):
+        loads[a].wait()
+        wait_all(outward, a)
+        if a == 0:
+            for copy in fetches:
+                copy.wait()
+        experts, many, _ = arrived[a].shape
+        rows = arrived[a][...].reshape(experts * many, features)
         gate = jnp.dot(rows, gate_ref[...], preferred_element_type=jnp.float32)
         upward = jnp.dot(rows, up_ref[...], preferred_element_type=jnp.float32)
         hidden = (gate / (1.0 + jnp.exp(-gate)) * upward).astype(jnp.bfloat16)
-        outs[a][...] = jnp.dot(
-            hidden, down_ref[...], preferred_element_type=jnp.float32
+
+        for i in range(features // tile):
+            part = slice(i * tile, (i + 1) * tile)
+            results[a][:, :, part] = (
+                jnp.dot(hidden, down_ref[:, part], preferred_element_type=jnp.float32)
+                .astype(jnp.bfloat16)
+                .reshape(experts, many, tile)
+            )
+        start_all(homeward, a)
+        keeps[a].start()
+
+    row = 0
+    for a in range(count):
+        keeps[a].wait()
+        wait_all(homeward, a)
+        experts, many, _ = returned[a].shape
+        span = slice(row, row + experts * many)
+
+        @pl.loop(0, features // tile)
+        def _(i):
+            part = pl.ds(pl.multiple_of(i * tile, tile), tile)
+            block = returned[a][:, :, part].reshape(experts * many, tile)
+            total = jnp.dot(high_ref[:, span], block, preferred_element_type=jnp.float32) + jnp.dot(
+                low_ref[:, span], block, preferred_element_type=jnp.float32
+            )
+            combined[:, part] = total if a == 0 else combined[:, part] + total
+
+        row += experts * many
+
+    @pl.loop(0, stream_ref.shape[0] // 16)
+    def _(i):
+        part = pl.ds(pl.multiple_of(i * 16, 16), 16)
+        out_ref[part] = (
+            stream_ref[part].astype(jnp.float32) + normed_token_rows(combined[part], gain_ref[...])
         ).astype(jnp.bfloat16)
 
 
-def serve(arrays, gate, up, down):
+def back(sent, gate, up, down, high, low, stream, gain):
+    axes = ("sp", "dp")
+    sizes = [lax.axis_size(a) for a in axes]
+    n = sent[0].shape[0]
+    count = len(sent)
+    whole, anywhere = pl.BlockSpec(memory_space=pltpu.VMEM), pl.BlockSpec(memory_space=pl.ANY)
+    dma = pltpu.SemaphoreType.DMA
     return pl.pallas_call(
-        functools.partial(expert_kernel, len(arrays)),
-        out_shape=[jax.ShapeDtypeStruct(a.shape, a.dtype) for a in arrays],
-        in_specs=[pl.BlockSpec(memory_space=pltpu.VMEM)] * (len(arrays) + 3),
-        out_specs=[pl.BlockSpec(memory_space=pltpu.VMEM)] * len(arrays),
-        compiler_params=pltpu.CompilerParams(vmem_limit_bytes=VMEM_LIMIT),
-    )(*arrays, gate, up, down)
-
-
-def combine_kernel(count, *refs):
-    ins = refs[:count]
-    high_ref, low_ref, stream_ref, gain_ref, out_ref = refs[count:]
-    combined, row = 0.0, 0
-    for ref in ins:
-        many = ref.shape[0]
-        for share in (high_ref, low_ref):
-            combined = combined + jnp.dot(
-                share[:, row : row + many], ref[...], preferred_element_type=jnp.float32
-            )
-        row += many
-    out_ref[...] = (
-        stream_ref[...].astype(jnp.float32) + normed_token_rows(combined, gain_ref[...])
-    ).astype(jnp.bfloat16)
-
-
-def combine(arrays, high, low, stream, gain):
-    return pl.pallas_call(
-        functools.partial(combine_kernel, len(arrays)),
-        out_shape=jax.ShapeDtypeStruct(stream.shape, jnp.bfloat16),
-        in_specs=[pl.BlockSpec(memory_space=pltpu.VMEM)] * (len(arrays) + 4),
-        out_specs=pl.BlockSpec(memory_space=pltpu.VMEM),
-        compiler_params=pltpu.CompilerParams(vmem_limit_bytes=VMEM_LIMIT),
-    )(*arrays, high, low, stream, gain[None])
+        functools.partial(back_kernel, axes, sizes, n, count),
+        out_shape=jax.ShapeDtypeStruct(stream.shape, stream.dtype),
+        in_specs=[anywhere] * (count + 3) + [whole] * 4,
+        out_specs=whole,
+        scratch_shapes=[pltpu.VMEM(a.shape, a.dtype) for _ in range(3) for a in sent]
+        + [pltpu.VMEM(w.shape, w.dtype) for w in (gate, up, down)]
+        + [pltpu.VMEM(stream.shape, jnp.float32)]
+        + [dma((count, n))] * 4
+        + [dma((2 * count,)), dma((3,))],
+        compiler_params=pltpu.CompilerParams(
+            collective_id=1, has_side_effects=True, vmem_limit_bytes=VMEM_LIMIT
+        ),
+    )(*sent, gate, up, down, high, low, stream, gain[None])
 
 
 def local(
@@ -513,8 +518,6 @@
 ):
     sp = lax.axis_size("sp")
     _, local_rows, heads, width = queries.shape
-    features = residual.shape[2]
-
     dp = lax.axis_size("dp")
     experts = sp * dp
     top_count = routes.shape[2]
@@ -531,7 +534,6 @@
     before = jnp.dot(earlier, onehot, preferred_element_type=jnp.float32)
     rank = jnp.sum(before * onehot.astype(jnp.float32), axis=1).astype(jnp.int32)
     groups = [g for g in (capacity // 8 * 8, capacity % 8) if g]
-    splits = [g * experts for g in groups]
     slot, first, base = jnp.full((count,), -1, jnp.int32), 0, 0
     for g in groups:
         inside = (rank >= first) & (rank < first + g)
@@ -549,16 +551,9 @@
         queries[0], key_rows[0], values[0], out_weight, residual[0], mixer_gain, expert_gain, pick, experts, groups
     )
 
-    def blocks(arrays):
-        return [a.reshape(experts, g, features) for a, g in zip(arrays, groups)]
-
-    def flat(arrays):
-        return [a.reshape(-1, features) for a in arrays]
-
-    arrived = exchange(outgoing, ("sp", "dp"), 2)
-    results = serve(flat(arrived), gate_weight[0], up_weight[0], expert_down_matrix[0])
-    returned = exchange(blocks(results), ("sp", "dp"), 3)
-    output = combine(flat(returned), share_high, share_low, stream, output_gain)
+    output = back(
+        outgoing, gate_weight[0], up_weight[0], expert_down_matrix[0], share_high, share_low, stream, output_gain
+    )
     return output[None]
 
 

time: 269 us -> 240 us (0.89)
  Pallas kernels: 259 us -> 234 us
  local copies, waits for them, and re-layouts: 7.67 us -> 4.17 us
    pallas_call x4 -> x1, Pallas kernels: 177 us -> 152 us  [back(): pl.pallas_call(functools.partial(back_kernel, axes, sizes, n, count), out...]
    reshape x3 -> x0, local copies, waits for them, and re-layouts: 6.54 us -> none  [the longest x2 4.29 us: flat(): return [a.reshape(-1, features) for a in arrays]]
where the time goes in v2:
time: 240 us
  Pallas kernels  234 us (98%)
  local copies, waits for them, and re-layouts  4.17 us (2%)
    pallas_call x1, Pallas kernels, back(): pl.pallas_call(functools.partial(back_kernel, axes, sizes, n, count), out...  152 us
    pallas_call x1, Pallas kernels, front(): pl.pallas_call(functools.partial(front_kernel, sp, dp, len(groups)), out_...  81.8 us

profile of v2, /device:TPU:16, one launch (start us, length us, event | category | flops | bytes accessed | tf_op | source)
XLA Modules:
  0.0 240.2 jit_solution(17083098575369800256)
XLA Ops:
  0.0 0.8 slice_bitcast_fusion.1
  0.8 0.8 copy.22
  1.5 0.1 eq.40
  1.7 0.2 fusion
  1.9 0.1 convert_element_type.30
  2.0 0.1 copy.23
  2.1 0.7 and_select_fusion.1
  2.8 0.7 fusion.3.refs_7_
  3.5 0.8 subtract_convert_fusion
  4.3 81.8 %shard_map.127 = (bf16[128,4096]{1,0:T(8,128)(2,1)}, bf16[32,8,4096]{2,1,0:T(8,128)(2,1)}, bf16[32,4,4096]{2,1,0:T(4,128)(2,1)}) custom-call(bf16[128,16,128]{2,1,0:T(8,128)(2,1)} %bitcast.35, bf16[128,16,128]{2,1,0:T(8,128)(2,1)} %bitcast.36, bf16[128,16,128]{2,1,0:T(8,128)(2,1)} %bitcast.37, bf16[2048,1024]{1,0:T(8,128)(2,1)} %refs_3_.1, ...), custom_call_target="tpu_custom_call" | custom-call | tf_op jit(solution)/shard_map/pallas_call | solution.py:328
  86.1 151.8 %shard_map.128 = bf16[128,4096]{1,0:T(8,128)(2,1)} custom-call(bf16[32,8,4096]{2,1,0:T(8,128)(2,1)} %get-tuple-element.8.refs_0_, bf16[32,4,4096]{2,1,0:T(4,128)(2,1)} %get-tuple-element.9.refs_1_, bf16[4096,512]{1,0:T(8,128)(2,1)} %bitcast.30, bf16[4096,512]{1,0:T(8,128)(2,1)} %bitcast.31, bf16[512,4096]{1,0:T(8,128)(2,1)} %bitcast.32, ...), custom_call_target="tpu_custom_call" | custom-call | tf_op jit(solution)/shard_map/pallas_call | solution.py:488
  237.9 2.3 copy.30
  (2 shorter events, 0.0 us)

commit v3 on v2

v3 whole, which is shorter than its diff:
```python
import functools

import jax
import jax.numpy as jnp
from jax import lax
from jax.experimental import pallas as pl
from jax.experimental.pallas import tpu as pltpu
from jax.sharding import PartitionSpec as P

EPSILON = 1e-06
MESH = pl.DeviceIdType.MESH
VMEM_LIMIT = 63 * 1024 * 1024


def normed_token_rows(matrix, gain):
    return matrix * lax.rsqrt(jnp.mean(matrix * matrix, axis=-1, keepdims=True) + EPSILON) * gain


CHUNKS = 8
RELAYED = 3
DIRECT = 2


def place_slots(rows, experts, groups, routes_ref, shares_ref, pick_ref, high_ref, low_ref):
    top_count = routes_ref.shape[0]

    def column(row):
        return jnp.transpose(jnp.broadcast_to(row, (rows, rows)))[:, :1]

    lanes = lax.broadcasted_iota(jnp.int32, (rows, max(experts, 128)), 1).astype(jnp.float32)
    names = [column(routes_ref[k : k + 1].astype(jnp.float32)) for k in range(top_count)]
    shares = [column(shares_ref[k : k + 1]) for k in range(top_count)]
    marks = [jnp.where(name == lanes, 1.0, 0.0) for name in names]
    earlier = lax.broadcasted_iota(jnp.int32, (rows, rows), 1) < lax.broadcasted_iota(jnp.int32, (rows, rows), 0)
    before = jnp.dot(
        jnp.where(earlier, 1.0, 0.0).astype(jnp.bfloat16),
        sum(marks).astype(jnp.bfloat16),
        preferred_element_type=jnp.float32,
    )
    slot_ids = lax.broadcasted_iota(jnp.int32, (rows, experts * sum(groups)), 1).astype(jnp.float32)
    picked, share = 0.0, 0.0
    for k in range(top_count):
        rank = jnp.sum(before * marks[k], axis=1, keepdims=True)
        slot, first, base = jnp.full((rows, 1), -1.0, jnp.float32), 0, 0
        for g in groups:
            inside = (rank >= first) & (rank < first + g)
            slot = jnp.where(inside, base + names[k] * g + rank - first, slot)
            first, base = first + g, base + g * experts
        picked = picked + jnp.where(slot == slot_ids, 1.0, 0.0)
        share = share + jnp.where(slot == slot_ids, shares[k], 0.0)
    pick_ref[...] = jnp.transpose(picked).astype(jnp.bfloat16)
    high = share.astype(jnp.bfloat16)
    high_ref[...] = high
    low_ref[...] = (share - high.astype(jnp.float32)).astype(jnp.bfloat16)


def layer_kernel(sp, dp, count, *refs):
    (
        q_ref, k_ref, v_ref, weight_ref, resid_ref, mixer_ref, expert_ref, routes_ref, shares_ref,
        gate_hbm, up_hbm, down_hbm, gain_ref, out_ref,
    ) = refs[:14]
    boxes = refs[14 : 14 + 4 * count]
    sent, served = boxes[:count], boxes[count : 2 * count]
    results, returned = boxes[2 * count : 3 * count], boxes[3 * count :]
    (
        stage, arrived, out_heads, in_heads, flat, full, projected, tokens, stream_ref,
        pick_ref, high_ref, low_ref, gate_ref, up_ref, down_ref,
        q_send, q_recv, a_send, a_recv, near_sem, far_send, far_recv, relay_send, relay_recv,
        twin_send, twin_recv, last_send, last_recv, local_sem,
        send_sem, recv_sem, back_send, back_recv, keep_sem, fetch_sem,
    ) = refs[14 + 4 * count :]
    rows, heads, width = q_ref.shape
    local_heads = heads // sp
    depth, columns = weight_ref.shape
    me, mate = lax.axis_index("sp"), lax.axis_index("dp")
    parity, core = lax.rem(me, 2), lax.rem(mate, 2)
    side, twin = me + 1 - 2 * parity, mate + 1 - 2 * core
    ys = dp // 2
    own_y = lax.div(mate, 2)
    n, own = sp * dp, me * dp + mate

    def signal(device):
        pl.semaphore_signal(barrier, inc=1, device_id=device, device_id_type=MESH)

    barrier = pltpu.get_barrier_semaphore()

    def greet(k, carry):
        other = lax.rem(own + k, n)
        signal({"sp": lax.div(other, dp), "dp": lax.rem(other, dp)})
        return carry

    lax.fori_loop(1, n, greet, 0)
    load = pltpu.make_async_copy(weight_ref, full.at[mate], local_sem.at[0])
    load.start()
    stage[0] = jnp.transpose(q_ref[...], (1, 0, 2))
    stage[1] = jnp.transpose(k_ref[...], (1, 0, 2))
    pl.semaphore_wait(barrier, n - 1)

    def head_copy(t, h, k):
        target = lax.rem(me + k, sp)
        return pltpu.make_async_remote_copy(
            src_ref=stage.at[t, target * local_heads + h],
            dst_ref=arrived.at[t, me, h],
            send_sem=q_send.at[t, h, k],
            recv_sem=q_recv.at[t, h, k],
            device_id={"sp": target},
            device_id_type=MESH,
        )

    def send_heads(t, h):
        def push(i, carry):
            k = sp // 2 + (1 - 2 * lax.rem(i, 2)) * lax.div(i + 1, 2)
            head_copy(t, h, k).start()
            return carry

        lax.fori_loop(0, sp - 1, push, 0)

    def finish(make, low, high):
        def body(k, carry):
            make(k).wait()
            return carry

        lax.fori_loop(low, high, body, 0)

    span = depth // CHUNKS

    def chunk(owner_parity, j):
        if j < RELAYED:
            return pl.ds(pl.multiple_of((owner_parity * (RELAYED + DIRECT) + j) * span, span), span)
        return pl.ds(j * span, span)

    def shift(src, dst, sends, recvs, index, device):
        return pltpu.make_async_remote_copy(
            src_ref=src, dst_ref=dst, send_sem=sends.at[index], recv_sem=recvs.at[index],
            device_id=device, device_id_type=MESH,
        )

    def far(d, j):
        where = chunk(parity, j)
        return shift(
            weight_ref.at[where], full.at[mate, where], far_send, far_recv, (d - 1, j),
            {"dp": lax.rem(own_y + d, ys) * 2 + core},
        )

    def relay(d, j):
        origin = lax.rem(own_y + ys - d, ys) * 2 + core
        where = chunk(parity, j)
        block = full.at[origin, where]
        return shift(block, block, relay_send, relay_recv, (d - 1, j), {"sp": side})

    def to_twin(d, j):
        origin = lax.rem(own_y + ys - d, ys) * 2 + core
        block = full.at[origin, chunk(parity, j)]
        return shift(block, block, twin_send, twin_recv, (d - 1, j), {"dp": twin})

    def to_twin_last(d, j):
        origin = lax.rem(own_y + ys - d, ys) * 2 + core
        block = full.at[origin, chunk(1 - parity, j)]
        return shift(block, block, last_send, last_recv, (d - 1, j), {"dp": twin})

    near = pltpu.make_async_remote_copy(
        src_ref=weight_ref, dst_ref=full.at[mate], send_sem=near_sem.at[0], recv_sem=near_sem.at[1],
        device_id={"dp": twin}, device_id_type=MESH,
    )
    for d in range(1, ys):
        far(d, 0).start()
    send_heads(0, 0)
    send_heads(1, 0)
    for d in range(1, ys):
        for j in range(1, RELAYED + DIRECT):
            far(d, j).start()
    near.start()
    stage[2] = jnp.transpose(v_ref[...], (1, 0, 2))
    keep_heads = [
        pltpu.make_async_copy(
            stage.at[t, pl.ds(me * local_heads, local_heads)], arrived.at[t, me], local_sem.at[1 + t]
        )
        for t in range(3)
    ]
    for copy in keep_heads[:2]:
        copy.start()
    fetches = [
        pltpu.make_async_copy(src, dst, fetch_sem.at[i])
        for i, (src, dst) in enumerate(((gate_hbm, gate_ref), (up_hbm, up_ref), (down_hbm, down_ref)))
    ]
    for copy in fetches:
        copy.start()
    send_heads(2, 0)
    keep_heads[2].start()
    for h in range(1, local_heads):
        for t in range(3):
            send_heads(t, h)

    place_slots(rows, n, [box.shape[1] for box in sent], routes_ref, shares_ref, pick_ref, high_ref, low_ref)

    block = rows * max(1, min(sp, 256 // rows))
    per = block // rows
    length = sp * rows
    scale = width ** (-0.5)
    tri_row = lax.broadcasted_iota(jnp.int32, (block, block), 0)
    tri_col = lax.broadcasted_iota(jnp.int32, (block, block), 1)
    suffix_ones = (tri_row >= tri_col).astype(jnp.bfloat16)
    is_past = tri_col < tri_row

    def answer(h, target):
        return pltpu.make_async_remote_copy(
            src_ref=out_heads.at[h, target],
            dst_ref=in_heads.at[me, h],
            send_sem=a_send.at[h, target],
            recv_sem=a_recv.at[h, me],
            device_id={"sp": target},
            device_id_type=MESH,
        )

    def expect(h, source):
        return pltpu.make_async_remote_copy(
            src_ref=out_heads.at[h, source],
            dst_ref=in_heads.at[source, h],
            send_sem=a_send.at[h, source],
            recv_sem=a_recv.at[h, source],
            device_id={"sp": source},
            device_id_type=MESH,
        )

    def attend_head(h):
        def piece(t, index):
            return arrived[t, index * per : (index + 1) * per, h].reshape(block, width)

        for q_block in range(length // block):
            query = piece(0, q_block)
            total = jnp.zeros((block, width), jnp.float32)
            later = jnp.zeros((block, 1), jnp.float32)
            for k_block in range(q_block, -1, -1):
                scores = (
                    lax.dot_general(
                        query, piece(1, k_block), (((1,), (1,)), ((), ())),
                        preferred_element_type=jnp.float32,
                    )
                    * scale
                )
                soft = jnp.maximum(scores, 0.0) + jnp.log(1.0 + jnp.exp(-jnp.abs(scores)))
                if k_block == q_block:
                    soft = jnp.where(is_past, soft, 0.0)
                high = soft.astype(jnp.bfloat16)
                low = (soft - high.astype(jnp.float32)).astype(jnp.bfloat16)
                suffix = jnp.dot(high, suffix_ones, preferred_element_type=jnp.float32) + jnp.dot(
                    low, suffix_ones, preferred_element_type=jnp.float32
                )
                weights = jnp.exp(scores - suffix - later)
                if k_block == q_block:
                    weights = jnp.where(is_past, weights, 0.0)
                total = total + jnp.dot(
                    weights.astype(jnp.bfloat16), piece(2, k_block), preferred_element_type=jnp.float32
                )
                if k_block > 0:
                    later = later + suffix[:, :1]
            out_heads[h, q_block * per : (q_block + 1) * per] = total.astype(jnp.bfloat16).reshape(
                per, rows, width
            )

    def send_answers(h):
        def push(k, carry):
            answer(h, lax.rem(me + k, sp)).start()
            return carry

        lax.fori_loop(1, sp, push, 0)
        pltpu.make_async_copy(out_heads.at[h, me], in_heads.at[me, h], local_sem.at[4 + h]).start()

    def pass_on(j):
        for d in range(1, ys):
            far(d, j).wait_recv()
            if j < RELAYED:
                relay(d, j).start()
            to_twin(d, j).start()

    def pass_last(j):
        for d in range(1, ys):
            pltpu.make_async_remote_copy(
                src_ref=full.at[0, chunk(1 - parity, j)],
                dst_ref=full.at[0, chunk(1 - parity, j)],
                send_sem=relay_send.at[d - 1, j], recv_sem=relay_recv.at[d - 1, j],
                device_id={"sp": side}, device_id_type=MESH,
            ).wait_recv()
            to_twin_last(d, j).start()

    pass_on(0)
    for h in range(local_heads):
        if h == 0:
            for copy in keep_heads:
                copy.wait()
        for t in range(3):
            finish(lambda k: head_copy(t, h, k), 1, sp)
        attend_head(h)
        send_answers(h)
        if h == 0:
            pass_on(1)
    pass_on(2)
    for j in range(RELAYED - 1):
        pass_last(j)
    pass_on(RELAYED)
    pass_last(RELAYED - 1)

    for h in range(local_heads):
        finish(lambda k: expect(h, lax.rem(me + k, sp)), 1, sp)
        pltpu.make_async_copy(out_heads.at[h, me], in_heads.at[me, h], local_sem.at[4 + h]).wait()
    for source in range(sp):
        for h in range(local_heads):
            place = (source * local_heads + h) * width
            flat[:, place : place + width] = in_heads[source, h]

    def settle(j):
        for d in range(1, ys):
            far(d, j).wait_send()
            to_twin(d, j).wait()
            if j < RELAYED:
                relay(d, j).wait_send()
                to_twin_last(d, j).wait()

    load.wait()
    near.wait()
    for j in range(RELAYED + DIRECT - 1):
        settle(j)

    tile = min(columns, 512)
    many = columns // tile
    late = (RELAYED + DIRECT - 1) * span
    after = late + span

    def project(combine):
        @pl.loop(0, dp * many)
        def _(i):
            inner = pl.ds(pl.multiple_of(lax.rem(i, many) * tile, tile), tile)
            outer = pl.ds(pl.multiple_of(i * tile, tile), tile)
            combine(lax.div(i, many), inner, outer)

    def early(owner, inner, outer):
        projected[:, outer] = jnp.dot(
            flat[:, :late], full[owner, :late, inner], preferred_element_type=jnp.float32
        ) + jnp.dot(flat[:, after:], full[owner, after:, inner], preferred_element_type=jnp.float32)

    def finally_add(owner, inner, outer):
        projected[:, outer] += jnp.dot(
            flat[:, late:after], full[owner, late:after, inner], preferred_element_type=jnp.float32
        )

    project(early)
    pass_on(RELAYED + DIRECT - 1)
    settle(RELAYED + DIRECT - 1)
    project(finally_add)

    @pl.loop(0, rows // 16)
    def _(i):
        part = pl.ds(pl.multiple_of(i * 16, 16), 16)
        stream = (
            resid_ref[part].astype(jnp.float32) + normed_token_rows(projected[part], mixer_ref[...])
        ).astype(jnp.bfloat16)
        stream_ref[part] = stream
        tokens[part] = normed_token_rows(stream.astype(jnp.float32), expert_ref[...]).astype(jnp.bfloat16)

    features = projected.shape[1]
    tile = 512

    def move(sources, targets, sends, recvs, a, target, slot):
        return pltpu.make_async_remote_copy(
            src_ref=sources[a].at[target],
            dst_ref=targets[a].at[own],
            send_sem=sends.at[a, target],
            recv_sem=recvs.at[a, slot],
            device_id={"sp": lax.div(target, dp), "dp": lax.rem(target, dp)},
            device_id_type=MESH,
        )

    def outward(a, target, slot):
        return move(sent, served, send_sem, recv_sem, a, target, slot)

    def homeward(a, target, slot):
        return move(results, returned, back_send, back_recv, a, target, slot)

    def start_all(make, a, first, number):
        def push(i, carry):
            target = first + lax.rem(lax.rem(own, number) + number // 2 + i, number)

            @pl.when(target != own)
            def _():
                make(a, target, own).start()

            return carry

        lax.fori_loop(0, number, push, 0)

    def wait_all(make, a):
        def body(k, carry):
            other = lax.rem(own + k, n)
            make(a, other, other).wait()
            return carry

        lax.fori_loop(1, n, body, 0)

    half = n // 2
    far_half = (1 - lax.div(own, half)) * half
    loads = [pltpu.make_async_copy(sent[a].at[own], served[a].at[own], keep_sem.at[a]) for a in range(count)]
    keeps = [
        pltpu.make_async_copy(results[a].at[own], returned[a].at[own], keep_sem.at[count + a])
        for a in range(count)
    ]
    row = 0
    for a in range(count):
        many = sent[a].shape[1]
        for first in (far_half, half - far_half):
            wanted = pick_ref[pl.ds(pl.multiple_of(row + first * many, half * many), half * many)]

            @pl.loop(0, features // tile)
            def _(i):
                part = pl.ds(pl.multiple_of(i * tile, tile), tile)
                sent[a][pl.ds(first, half), :, part] = (
                    jnp.dot(wanted, tokens[:, part], preferred_element_type=jnp.float32)
                    .astype(jnp.bfloat16)
                    .reshape(half, many, tile)
                )

            start_all(outward, a, first, half)
        loads[a].start()
        row += n * many

    for a in range(count):
        loads[a].wait()
        wait_all(outward, a)
        if a == 0:
            for copy in fetches:
                copy.wait()
        many = served[a].shape[1]
        taken = served[a][...].reshape(n * many, features)
        gate = jnp.dot(taken, gate_ref[...], preferred_element_type=jnp.float32)
        upward = jnp.dot(taken, up_ref[...], preferred_element_type=jnp.float32)
        hidden = (gate / (1.0 + jnp.exp(-gate)) * upward).astype(jnp.bfloat16)
        for i in range(features // tile):
            part = slice(i * tile, (i + 1) * tile)
            results[a][:, :, part] = (
                jnp.dot(hidden, down_ref[:, part], preferred_element_type=jnp.float32)
                .astype(jnp.bfloat16)
                .reshape(n, many, tile)
            )
        start_all(homeward, a, far_half, half)
        start_all(homeward, a, half - far_half, half)
        keeps[a].start()

    row = 0
    for a in range(count):
        keeps[a].wait()
        wait_all(homeward, a)
        many = returned[a].shape[1]
        columns_of = slice(row, row + n * many)

        @pl.loop(0, features // tile)
        def _(i):
            part = pl.ds(pl.multiple_of(i * tile, tile), tile)
            block = returned[a][:, :, part].reshape(n * many, tile)
            total = jnp.dot(high_ref[:, columns_of], block, preferred_element_type=jnp.float32) + jnp.dot(
                low_ref[:, columns_of], block, preferred_element_type=jnp.float32
            )
            projected[:, part] = total if a == 0 else projected[:, part] + total

        row += n * many

    @pl.loop(0, rows // 16)
    def _(i):
        part = pl.ds(pl.multiple_of(i * 16, 16), 16)
        out_ref[part] = (
            stream_ref[part].astype(jnp.float32) + normed_token_rows(projected[part], gain_ref[...])
        ).astype(jnp.bfloat16)


def layer(
    query, key, value, weight, residual, mixer_gain, expert_gain, routes, shares, gate, up, down, gain, groups
):
    sp, dp = lax.axis_size("sp"), lax.axis_size("dp")
    n = sp * dp
    rows, heads, width = query.shape
    depth, columns = weight.shape
    features = residual.shape[1]
    local_heads = heads // sp
    ys = max(dp // 2 - 1, 1)
    slots = n * sum(groups)
    whole, anywhere = pl.BlockSpec(memory_space=pltpu.VMEM), pl.BlockSpec(memory_space=pl.ANY)
    dma = pltpu.SemaphoreType.DMA
    bf16 = jnp.bfloat16
    return pl.pallas_call(
        functools.partial(layer_kernel, sp, dp, len(groups)),
        out_shape=jax.ShapeDtypeStruct((rows, features), bf16),
        in_specs=[whole] * 3 + [anywhere] + [whole] * 5 + [anywhere] * 3 + [whole],
        out_specs=whole,
        scratch_shapes=[pltpu.VMEM((n, g, features), bf16) for _ in range(4) for g in groups]
        + [
            pltpu.VMEM((3, heads, rows, width), bf16),
            pltpu.VMEM((3, sp, local_heads, rows, width), bf16),
            pltpu.VMEM((local_heads, sp, rows, width), bf16),
            pltpu.VMEM((sp, local_heads, rows, width), bf16),
            pltpu.VMEM((rows, depth), bf16),
            pltpu.VMEM((dp, depth, columns), bf16),
            pltpu.VMEM((rows, features), jnp.float32),
            pltpu.VMEM((rows, features), bf16),
            pltpu.VMEM((rows, features), bf16),
            pltpu.VMEM((slots, rows), bf16),
            pltpu.VMEM((rows, slots), bf16),
            pltpu.VMEM((rows, slots), bf16),
            pltpu.VMEM(gate.shape, bf16),
            pltpu.VMEM(up.shape, bf16),
            pltpu.VMEM(down.shape, bf16),
            dma((3, local_heads, sp)),
            dma((3, local_heads, sp)),
            dma((local_heads, sp)),
            dma((local_heads, sp)),
            dma((2,)),
            dma((ys, RELAYED + DIRECT)),
            dma((ys, RELAYED + DIRECT)),
            dma((ys, RELAYED)),
            dma((ys, RELAYED)),
            dma((ys, RELAYED + DIRECT)),
            dma((ys, RELAYED + DIRECT)),
            dma((ys, RELAYED)),
            dma((ys, RELAYED)),
            dma((4 + local_heads,)),
            dma((len(groups), n)),
            dma((len(groups), n)),
            dma((len(groups), n)),
            dma((len(groups), n)),
            dma((2 * len(groups),)),
            dma((3,)),
        ],
        compiler_params=pltpu.CompilerParams(
            collective_id=0, has_side_effects=True, vmem_limit_bytes=VMEM_LIMIT
        ),
    )(
        query, key, value, weight, residual, mixer_gain[None], expert_gain[None], routes, shares,
        gate, up, down, gain[None],
    )


def local(
    queries,
    key_rows,
    values,
    residual,
    out_weight,
    mixer_gain,
    expert_gain,
    gate_weight,
    up_weight,
    expert_down_matrix,
    routes,
    route_weight,
    output_gain,
):
    local_rows = queries.shape[1]
    experts = lax.axis_size("sp") * lax.axis_size("dp")
    capacity = max(2, 3 * local_rows // experts)
    groups = [g for g in (capacity // 8 * 8, capacity % 8) if g]
    output = layer(
        queries[0], key_rows[0], values[0], out_weight, residual[0], mixer_gain, expert_gain,
        routes[0].T, route_weight[0].T, gate_weight[0], up_weight[0], expert_down_matrix[0], output_gain, groups,
    )
    return output[None]


def solution(mesh):
    in_specs = (
        P("dp", "sp", None, None),
        P("dp", "sp", None, None),
        P("dp", "sp", None, None),
        P("dp", "sp", None),
        P(None, "dp"),
        P(),
        P(),
        P(("sp", "dp"), None, None),
        P(("sp", "dp"), None, None),
        P(("sp", "dp"), None, None),
        P("dp", "sp", None),
        P("dp", "sp", None),
        P(),
    )
    out_specs = P("dp", "sp", None)
    return jax.shard_map(local, mesh=mesh, in_specs=in_specs, out_specs=out_specs, check_vma=False)
```

time: 240 us -> 238 us (level); the launches traced: 240 us -> 235 us
    pallas_call x2 -> x1, Pallas kernels: 234 us -> 233 us  [layer(): pl.pallas_call(functools.partial(layer_kernel, sp, dp, len(groups)), out_...]
where the time goes in v3:
time: 238 us; the launch traced here: 235 us
  Pallas kernels  233 us (98%)
    pallas_call x1, Pallas kernels, layer(): pl.pallas_call(functools.partial(layer_kernel, sp, dp, len(groups)), out_...  233 us

profile of v3, /device:TPU:16, one launch (start us, length us, event | category | flops | bytes accessed | tf_op | source)
XLA Modules:
  0.0 235.4 jit_solution(11105899987627237050)
XLA Ops:
  0.0 233.1 %shard_map.127 = bf16[128,4096]{1,0:T(8,128)(2,1)} custom-call(bf16[128,16,128]{2,1,0:T(8,128)(2,1)} %bitcast.22, bf16[128,16,128]{2,1,0:T(8,128)(2,1)} %bitcast.23, bf16[128,16,128]{2,1,0:T(8,128)(2,1)} %bitcast.24, bf16[2048,1024]{1,0:T(8,128)(2,1)} %refs_3_.1, bf16[128,4096]{1,0:T(8,128)(2,1)} %bitcast.21, f32[1,4096]{1,0:T(1,128)} %bitcast.25, ...), custom_call_target="tpu_custom_call" | custom-call | tf_op jit(solution)/shard_map/pallas_call | solution.py:487
  233.1 2.3 copy.15

commit v4 on v3

v4 whole, which is shorter than its diff:
```python
import functools

import jax
import jax.numpy as jnp
from jax import lax
from jax.experimental import pallas as pl
from jax.experimental.pallas import tpu as pltpu
from jax.sharding import PartitionSpec as P

EPSILON = 1e-06
MESH = pl.DeviceIdType.MESH
VMEM_LIMIT = 60 * 1024 * 1024


def normed_token_rows(matrix, gain):
    return matrix * lax.rsqrt(jnp.mean(matrix * matrix, axis=-1, keepdims=True) + EPSILON) * gain


PIECES = 2


def place_slots(rows, experts, groups, routes_ref, shares_ref, pick_ref, high_ref, low_ref):
    top_count = routes_ref.shape[0]

    def column(row):
        return jnp.transpose(jnp.broadcast_to(row, (rows, rows)))[:, :1]

    lanes = lax.broadcasted_iota(jnp.int32, (rows, max(experts, 128)), 1).astype(jnp.float32)
    names = [column(routes_ref[k : k + 1].astype(jnp.float32)) for k in range(top_count)]
    shares = [column(shares_ref[k : k + 1]) for k in range(top_count)]
    marks = [jnp.where(name == lanes, 1.0, 0.0) for name in names]
    earlier = lax.broadcasted_iota(jnp.int32, (rows, rows), 1) < lax.broadcasted_iota(jnp.int32, (rows, rows), 0)
    before = jnp.dot(
        jnp.where(earlier, 1.0, 0.0).astype(jnp.bfloat16),
        sum(marks).astype(jnp.bfloat16),
        preferred_element_type=jnp.float32,
    )
    slot_ids = lax.broadcasted_iota(jnp.int32, (rows, experts * sum(groups)), 1).astype(jnp.float32)
    picked, share = 0.0, 0.0
    for k in range(top_count):
        rank = jnp.sum(before * marks[k], axis=1, keepdims=True)
        slot, first, base = jnp.full((rows, 1), -1.0, jnp.float32), 0, 0
        for g in groups:
            inside = (rank >= first) & (rank < first + g)
            slot = jnp.where(inside, base + names[k] * g + rank - first, slot)
            first, base = first + g, base + g * experts
        picked = picked + jnp.where(slot == slot_ids, 1.0, 0.0)
        share = share + jnp.where(slot == slot_ids, shares[k], 0.0)
    pick_ref[...] = jnp.transpose(picked).astype(jnp.bfloat16)
    high = share.astype(jnp.bfloat16)
    high_ref[...] = high
    low_ref[...] = (share - high.astype(jnp.float32)).astype(jnp.bfloat16)


def layer_kernel(sp, dp, count, *refs):
    (
        q_hbm, k_hbm, v_hbm, weight_ref, resid_hbm, mixer_hbm, expert_hbm, routes_hbm, shares_hbm,
        gate_hbm, up_hbm, down_hbm, gain_hbm, out_ref,
    ) = refs[:14]
    boxes = refs[14 : 14 + 4 * count]
    sent, served = boxes[:count], boxes[count : 2 * count]
    results, returned = boxes[2 * count : 3 * count], boxes[3 * count :]
    (
        raw, resid_ref, mixer_ref, expert_ref, gain_ref, routes_ref, shares_ref,
        stage, arrived, out_heads, in_heads, side_heads, flat, full, side_out, side_in,
        projected, tokens, stream_ref, pick_ref, high_ref, low_ref, gate_ref, up_ref, down_ref,
        load_sem, q_send, q_recv, a_send, a_recv, pass_send, pass_recv, near_sem, far_send, far_recv,
        twin_send, twin_recv, side_send, side_recv, local_sem,
        send_sem, recv_sem, back_send, back_recv, keep_sem, fetch_sem,
    ) = refs[14 + 4 * count :]
    _, rows, heads, width = raw.shape
    local_heads = heads // sp
    depth, columns = weight_ref.shape
    me, mate = lax.axis_index("sp"), lax.axis_index("dp")
    parity, core = lax.rem(me, 2), lax.rem(mate, 2)
    side, twin = me + 1 - 2 * parity, mate + 1 - 2 * core
    ys = dp // 2
    own_y = lax.div(mate, 2)
    n, own = sp * dp, me * dp + mate

    barrier = pltpu.get_barrier_semaphore()

    def greet(k, carry):
        other = lax.rem(own + k, n)
        pl.semaphore_signal(
            barrier, inc=1, device_id={"sp": lax.div(other, dp), "dp": lax.rem(other, dp)}, device_id_type=MESH
        )
        return carry

    lax.fori_loop(1, n, greet, 0)
    pairs = [
        (q_hbm, raw.at[0]), (k_hbm, raw.at[1]), (v_hbm, raw.at[2]), (routes_hbm, routes_ref),
        (shares_hbm, shares_ref), (weight_ref, full.at[core]), (resid_hbm, resid_ref), (mixer_hbm, mixer_ref),
        (expert_hbm, expert_ref), (gain_hbm, gain_ref),
    ]
    loads = [pltpu.make_async_copy(src, dst, load_sem.at[i]) for i, (src, dst) in enumerate(pairs)]
    for load in loads:
        load.start()
    for t in range(3):
        loads[t].wait()
        stage[t] = jnp.transpose(raw[t], (1, 0, 2))
    pl.semaphore_wait(barrier, n - 1)

    def await_bytes(ref, sem):
        pltpu.make_async_copy(ref, ref, sem).wait()

    def remote(src, dst, send, recv, device):
        return pltpu.make_async_remote_copy(
            src_ref=src, dst_ref=dst, send_sem=send, recv_sem=recv, device_id=device, device_id_type=MESH
        )

    def send_heads(t, h):
        def push(i, carry):
            k = sp // 2 + (1 - 2 * lax.rem(i, 2)) * lax.div(i + 1, 2)
            target = lax.rem(me + k, sp)
            remote(
                stage.at[t, target * local_heads + h], arrived.at[t, h, me], q_send.at[h], q_recv.at[h],
                {"sp": target},
            ).start()
            return carry

        lax.fori_loop(0, sp - 1, push, 0)

    others = pl.ds(0, sp - 1)
    span = depth // 2 // PIECES

    def piece_rows(owner, j):
        return pl.ds(pl.multiple_of(owner * (depth // 2) + j * span, span), span)

    def far(d, owner, j):
        where = piece_rows(owner, j)
        return remote(
            weight_ref.at[where], full.at[1 + d, where], far_send.at[d - 1, owner, j], far_recv.at[d - 1, j],
            {"dp": lax.rem(own_y + d, ys) * 2 + owner},
        )

    def far_in(d, j):
        where = full.at[1 + d, piece_rows(core, j)]
        return remote(where, where, far_send.at[d - 1, 0, j], far_recv.at[d - 1, j], {"dp": twin})

    def to_twin(d, j):
        where = full.at[1 + d, piece_rows(core, j)]
        return remote(where, where, twin_send.at[d - 1, j], twin_recv.at[d - 1, j], {"dp": twin})

    near = remote(weight_ref, full.at[core], near_sem.at[0], near_sem.at[1], {"dp": twin})
    for t in range(3):
        send_heads(t, 0)

    @pl.when(core == parity)
    def _():
        for j in range(PIECES):
            for d in range(1, ys):
                for owner in range(2):
                    far(d, owner, j).start()

    near.start()
    keep_heads = [
        pltpu.make_async_copy(stage.at[t, me * local_heads + h], arrived.at[t, h, me], local_sem.at[t, h])
        for t in range(3)
        for h in range(local_heads)
    ]
    for copy in keep_heads:
        copy.start()
    for h in range(1, local_heads):
        for t in range(3):
            send_heads(t, h)
    fetches = [
        pltpu.make_async_copy(src, dst, fetch_sem.at[i])
        for i, (src, dst) in enumerate(((gate_hbm, gate_ref), (up_hbm, up_ref), (down_hbm, down_ref)))
    ]
    for copy in fetches:
        copy.start()
    loads[3].wait()
    loads[4].wait()
    place_slots(rows, n, [box.shape[1] for box in sent], routes_ref, shares_ref, pick_ref, high_ref, low_ref)

    block = rows * max(1, min(sp, 256 // rows))
    per = block // rows
    length = sp * rows
    scale = width ** (-0.5)
    tri_row = lax.broadcasted_iota(jnp.int32, (block, block), 0)
    tri_col = lax.broadcasted_iota(jnp.int32, (block, block), 1)
    suffix_ones = (tri_row >= tri_col).astype(jnp.bfloat16)
    is_past = tri_col < tri_row

    def answer(h, target):
        return remote(
            out_heads.at[h, target], in_heads.at[h, me], a_send.at[h], a_recv.at[h, me], {"sp": target}
        )

    def expect(h, source):
        return remote(
            out_heads.at[h, source], in_heads.at[h, source], a_send.at[h], a_recv.at[h, source], {"sp": source}
        )

    def hand_on(h, source):
        return remote(
            in_heads.at[h, source], side_heads.at[h, source], pass_send.at[h], pass_recv.at[h], {"sp": side}
        )

    def attend_head(h):
        def piece(t, index):
            return arrived[t, h, index * per : (index + 1) * per].reshape(block, width)

        for q_block in range(length // block):
            query = piece(0, q_block)
            total = jnp.zeros((block, width), jnp.float32)
            later = jnp.zeros((block, 1), jnp.float32)
            for k_block in range(q_block, -1, -1):
                scores = (
                    lax.dot_general(
                        query, piece(1, k_block), (((1,), (1,)), ((), ())),
                        preferred_element_type=jnp.float32,
                    )
                    * scale
                )
                soft = jnp.maximum(scores, 0.0) + jnp.log(1.0 + jnp.exp(-jnp.abs(scores)))
                if k_block == q_block:
                    soft = jnp.where(is_past, soft, 0.0)
                high = soft.astype(jnp.bfloat16)
                low = (soft - high.astype(jnp.float32)).astype(jnp.bfloat16)
                suffix = jnp.dot(high, suffix_ones, preferred_element_type=jnp.float32) + jnp.dot(
                    low, suffix_ones, preferred_element_type=jnp.float32
                )
                weights = jnp.exp(scores - suffix - later)
                if k_block == q_block:
                    weights = jnp.where(is_past, weights, 0.0)
                total = total + jnp.dot(
                    weights.astype(jnp.bfloat16), piece(2, k_block), preferred_element_type=jnp.float32
                )
                if k_block > 0:
                    later = later + suffix[:, :1]
            out_heads[h, q_block * per : (q_block + 1) * per] = total.astype(jnp.bfloat16).reshape(
                per, rows, width
            )

    def send_answers(h):
        def push(k, carry):
            answer(h, lax.rem(me + k, sp)).start()
            return carry

        lax.fori_loop(1, sp, push, 0)
        keep_answer(h).start()

    def keep_answer(h):
        return pltpu.make_async_copy(out_heads.at[h, me], in_heads.at[h, me], local_sem.at[3, h])

    def pass_on(j):
        for d in range(1, ys):
            far_in(d, j).wait_recv()
            to_twin(d, j).start()

    for copy in keep_heads:
        copy.wait()
    for h in range(local_heads):
        await_bytes(arrived.at[:, h, others], q_recv.at[h])
        attend_head(h)
        send_answers(h)
    for j in range(PIECES - 1):
        pass_on(j)
    for h in range(local_heads):
        keep_answer(h).wait()
        hand_on(h, me).start()

        def follow(k, carry):
            source = lax.rem(me + k, sp)
            expect(h, source).wait_recv()
            hand_on(h, source).start()
            return carry

        lax.fori_loop(1, sp, follow, 0)
    pass_on(PIECES - 1)

    def fill(ref, first):
        for source in range(sp):
            for h in range(local_heads):
                place = (source * local_heads + h) * width
                flat[first : first + rows, place : place + width] = ref[h, source]

    fill(in_heads, 0)
    for h in range(local_heads):
        await_bytes(side_heads.at[h], pass_recv.at[h])
    fill(side_heads, rows)
    for d in range(1, ys):
        for j in range(PIECES):
            to_twin(d, j).wait()

    tile = min(columns, 512)
    many = columns // tile

    def split(i):
        return lax.div(i, many), pl.ds(pl.multiple_of(lax.rem(i, many) * tile, tile), tile)

    def place_of(slice_index, i):
        return pl.ds(pl.multiple_of((slice_index * many + lax.rem(i, many)) * tile, tile), tile)

    def hand_back(d):
        return remote(
            side_out.at[d - 1], side_in.at[d - 1], side_send.at[d - 1], side_recv.at[d - 1], {"sp": side}
        )

    for d in range(1, ys):

        @pl.loop(0, many)
        def _(i):
            _, inner = split(i)
            both = jnp.dot(flat[...], full[1 + d, :, inner], preferred_element_type=jnp.float32)
            projected[:, place_of(lax.rem(own_y + ys - d, ys) * 2 + parity, i)] = both[:rows]
            side_out[d - 1, :, inner] = both[rows:].astype(jnp.bfloat16)

        hand_back(d).start()

    loads[5].wait()
    near.wait()

    @pl.loop(0, 2 * many)
    def _(i):
        which, inner = split(i)
        projected[:, place_of(own_y * 2 + which, i)] = jnp.dot(
            flat[:rows], full[which, :, inner], preferred_element_type=jnp.float32
        )

    for load in loads[6:]:
        load.wait()
    for h in range(local_heads):
        await_bytes(stage.at[:, others], q_send.at[h])
        await_bytes(out_heads.at[h, others], a_send.at[h])
        await_bytes(in_heads.at[h], pass_send.at[h])

    @pl.when(core == parity)
    def _():
        for j in range(PIECES):
            for d in range(1, ys):
                for owner in range(2):
                    far(d, owner, j).wait_send()

    for d in range(1, ys):
        hand_back(d).wait()

        @pl.loop(0, many)
        def _(i):
            _, inner = split(i)
            projected[:, place_of(lax.rem(own_y + ys - d, ys) * 2 + 1 - parity, i)] = side_in[
                d - 1, :, inner
            ].astype(jnp.float32)

    @pl.loop(0, rows // 16)
    def _(i):
        part = pl.ds(pl.multiple_of(i * 16, 16), 16)
        stream = (
            resid_ref[part].astype(jnp.float32) + normed_token_rows(projected[part], mixer_ref[...])
        ).astype(jnp.bfloat16)
        stream_ref[part] = stream
        tokens[part] = normed_token_rows(stream.astype(jnp.float32), expert_ref[...]).astype(jnp.bfloat16)

    features = projected.shape[1]
    tile = 512

    def move(sources, targets, sends, recvs, a, target):
        return remote(
            sources[a].at[target], targets[a].at[own], sends.at[a], recvs.at[a],
            {"sp": lax.div(target, dp), "dp": lax.rem(target, dp)},
        )

    def outward(a, target):
        return move(sent, served, send_sem, recv_sem, a, target)

    def homeward(a, target):
        return move(results, returned, back_send, back_recv, a, target)

    def start_all(make, a, first, number):
        def push(i, carry):
            target = first + lax.rem(lax.rem(own, number) + number // 2 + i, number)

            @pl.when(target != own)
            def _():
                make(a, target).start()

            return carry

        lax.fori_loop(0, number, push, 0)

    peers = pl.ds(0, n - 1)
    half = n // 2
    far_half = (1 - lax.div(own, half)) * half
    own_rows = [pltpu.make_async_copy(sent[a].at[own], served[a].at[own], keep_sem.at[a]) for a in range(count)]
    keeps = [
        pltpu.make_async_copy(results[a].at[own], returned[a].at[own], keep_sem.at[count + a])
        for a in range(count)
    ]
    row = 0
    for a in range(count):
        many = sent[a].shape[1]
        for first in (far_half, half - far_half):
            wanted = pick_ref[pl.ds(pl.multiple_of(row + first * many, half * many), half * many)]

            @pl.loop(0, features // tile)
            def _(i):
                part = pl.ds(pl.multiple_of(i * tile, tile), tile)
                sent[a][pl.ds(first, half), :, part] = (
                    jnp.dot(wanted, tokens[:, part], preferred_element_type=jnp.float32)
                    .astype(jnp.bfloat16)
                    .reshape(half, many, tile)
                )

            start_all(outward, a, first, half)
        own_rows[a].start()
        row += n * many

    for a in range(count):
        own_rows[a].wait()
        await_bytes(served[a].at[peers], recv_sem.at[a])
        if a == 0:
            for copy in fetches:
                copy.wait()
        many = served[a].shape[1]
        taken = served[a][...].reshape(n * many, features)
        gate = jnp.dot(taken, gate_ref[...], preferred_element_type=jnp.float32)
        upward = jnp.dot(taken, up_ref[...], preferred_element_type=jnp.float32)
        hidden = (gate / (1.0 + jnp.exp(-gate)) * upward).astype(jnp.bfloat16)
        for i in range(features // tile):
            part = slice(i * tile, (i + 1) * tile)
            results[a][:, :, part] = (
                jnp.dot(hidden, down_ref[:, part], preferred_element_type=jnp.float32)
                .astype(jnp.bfloat16)
                .reshape(n, many, tile)
            )
        start_all(homeward, a, far_half, half)
        start_all(homeward, a, half - far_half, half)
        keeps[a].start()

    row = 0
    for a in range(count):
        keeps[a].wait()
        await_bytes(returned[a].at[peers], back_recv.at[a])
        many = returned[a].shape[1]
        columns_of = slice(row, row + n * many)

        @pl.loop(0, features // tile)
        def _(i):
            part = pl.ds(pl.multiple_of(i * tile, tile), tile)
            block = returned[a][:, :, part].reshape(n * many, tile)
            total = jnp.dot(high_ref[:, columns_of], block, preferred_element_type=jnp.float32) + jnp.dot(
                low_ref[:, columns_of], block, preferred_element_type=jnp.float32
            )
            projected[:, part] = total if a == 0 else projected[:, part] + total

        row += n * many

    for a in range(count):
        await_bytes(sent[a].at[peers], send_sem.at[a])
        await_bytes(results[a].at[peers], back_send.at[a])

    @pl.loop(0, rows // 16)
    def _(i):
        part = pl.ds(pl.multiple_of(i * 16, 16), 16)
        out_ref[part] = (
            stream_ref[part].astype(jnp.float32) + normed_token_rows(projected[part], gain_ref[...])
        ).astype(jnp.bfloat16)


def layer(
    query, key, value, weight, residual, mixer_gain, expert_gain, routes, shares, gate, up, down, gain, groups
):
    sp, dp = lax.axis_size("sp"), lax.axis_size("dp")
    n = sp * dp
    rows, heads, width = query.shape
    depth, columns = weight.shape
    features = residual.shape[1]
    local_heads = heads // sp
    extra = max(dp // 2 - 1, 1)
    slots = n * sum(groups)
    anywhere = pl.BlockSpec(memory_space=pl.ANY)
    dma = pltpu.SemaphoreType.DMA
    bf16, f32 = jnp.bfloat16, jnp.float32
    return pl.pallas_call(
        functools.partial(layer_kernel, sp, dp, len(groups)),
        out_shape=pltpu.VMEM((rows, features), bf16),
        in_specs=[anywhere] * 13,
        out_specs=pl.BlockSpec(memory_space=pltpu.VMEM),
        scratch_shapes=[pltpu.VMEM((n, g, features), bf16) for _ in range(4) for g in groups]
        + [
            pltpu.VMEM((3, rows, heads, width), bf16),
            pltpu.VMEM((rows, features), bf16),
            pltpu.VMEM((1, features), f32),
            pltpu.VMEM((1, features), f32),
            pltpu.VMEM((1, features), f32),
            pltpu.VMEM(routes.shape, jnp.int32),
            pltpu.VMEM(shares.shape, f32),
            pltpu.VMEM((3, heads, rows, width), bf16),
            pltpu.VMEM((3, local_heads, sp, rows, width), bf16),
            pltpu.VMEM((local_heads, sp, rows, width), bf16),
            pltpu.VMEM((local_heads, sp, rows, width), bf16),
            pltpu.VMEM((local_heads, sp, rows, width), bf16),
            pltpu.VMEM((2 * rows, depth), bf16),
            pltpu.VMEM((2 + extra, depth, columns), bf16),
            pltpu.VMEM((extra, rows, columns), bf16),
            pltpu.VMEM((extra, rows, columns), bf16),
            pltpu.VMEM((rows, features), f32),
            pltpu.VMEM((rows, features), bf16),
            pltpu.VMEM((rows, features), bf16),
            pltpu.VMEM((slots, rows), bf16),
            pltpu.VMEM((rows, slots), bf16),
            pltpu.VMEM((rows, slots), bf16),
            pltpu.VMEM(gate.shape, bf16),
            pltpu.VMEM(up.shape, bf16),
            pltpu.VMEM(down.shape, bf16),
            dma((10,)),
            dma((local_heads,)),
            dma((local_heads,)),
            dma((local_heads,)),
            dma((local_heads, sp)),
            dma((local_heads,)),
            dma((local_heads,)),
            dma((2,)),
            dma((extra, 2, PIECES)),
            dma((extra, PIECES)),
            dma((extra, PIECES)),
            dma((extra, PIECES)),
            dma((extra,)),
            dma((extra,)),
            dma((4, local_heads)),
            dma((len(groups),)),
            dma((len(groups),)),
            dma((len(groups),)),
            dma((len(groups),)),
            dma((2 * len(groups),)),
            dma((3,)),
        ],
        compiler_params=pltpu.CompilerParams(
            collective_id=0, has_side_effects=True, vmem_limit_bytes=VMEM_LIMIT
        ),
    )(
        query, key, value, weight, residual, mixer_gain[None], expert_gain[None], routes, shares,
        gate, up, down, gain[None],
    )


def local(
    queries,
    key_rows,
    values,
    residual,
    out_weight,
    mixer_gain,
    expert_gain,
    gate_weight,
    up_weight,
    expert_down_matrix,
    routes,
    route_weight,
    output_gain,
):
    local_rows = queries.shape[1]
    experts = lax.axis_size("sp") * lax.axis_size("dp")
    capacity = max(2, 3 * local_rows // experts)
    groups = [g for g in (capacity // 8 * 8, capacity % 8) if g]
    output = layer(
        queries[0], key_rows[0], values[0], out_weight, residual[0], mixer_gain, expert_gain,
        routes[0].T, route_weight[0].T, gate_weight[0], up_weight[0], expert_down_matrix[0], output_gain, groups,
    )
    return output[None]


def solution(mesh):
    in_specs = (
        P("dp", "sp", None, None),
        P("dp", "sp", None, None),
        P("dp", "sp", None, None),
        P("dp", "sp", None),
        P(None, "dp"),
        P(),
        P(),
        P(("sp", "dp"), None, None),
        P(("sp", "dp"), None, None),
        P(("sp", "dp"), None, None),
        P("dp", "sp", None),
        P("dp", "sp", None),
        P(),
    )
    out_specs = P("dp", "sp", None)
    return jax.shard_map(local, mesh=mesh, in_specs=in_specs, out_specs=out_specs, check_vma=False)
```

time: 238 us -> 220 us (0.924)
  Pallas kernels: 233 us -> 217 us
    pallas_call x1, Pallas kernels: 233 us -> 217 us  [layer(): pl.pallas_call(functools.partial(layer_kernel, sp, dp, len(groups)), out_...]
where the time goes in v4:
time: 220 us; the launch traced here: 218 us
  Pallas kernels  217 us (99%)
    pallas_call x1, Pallas kernels, layer(): pl.pallas_call(functools.partial(layer_kernel, sp, dp, len(groups)), out_...  217 us

profile of v4, /device:TPU:16, one launch (start us, length us, event | category | flops | bytes accessed | tf_op | source)
XLA Modules:
  0.0 217.9 jit_solution(16316268320610402249)
XLA Ops:
  0.0 216.9 %shard_map.127 = bf16[128,4096]{1,0:T(8,128)(2,1)S(1)} custom-call(bf16[128,16,128]{2,1,0:T(8,128)(2,1)} %bitcast.22, bf16[128,16,128]{2,1,0:T(8,128)(2,1)} %bitcast.23, bf16[128,16,128]{2,1,0:T(8,128)(2,1)} %bitcast.24, bf16[2048,1024]{1,0:T(8,128)(2,1)} %refs_3_.1, bf16[128,4096]{1,0:T(8,128)(2,1)} %bitcast.21, f32[1,4096]{1,0:T(1,128)} %bitcast.25, ...), custom_call_target="tpu_custom_call" | custom-call | tf_op jit(solution)/shard_map/pallas_call | solution.py:476
  216.9 1.0 copy.15

commit v5 on v4

--- a/solution.py
+++ b/solution.py
@@ -9,7 +9,7 @@
 
 EPSILON = 1e-06
 MESH = pl.DeviceIdType.MESH
-VMEM_LIMIT = 60 * 1024 * 1024
+VMEM_LIMIT = 62 * 1024 * 1024
 
 
 def normed_token_rows(matrix, gain):
@@ -19,8 +19,9 @@
 PIECES = 2
 
 
-def place_slots(rows, experts, groups, routes_ref, shares_ref, pick_ref, high_ref, low_ref):
+def place_slots(rows, experts, groups, halves, routes_ref, shares_ref, pick_refs, high_refs, low_refs):
     top_count = routes_ref.shape[0]
+    half = experts // 2
 
     def column(row):
         return jnp.transpose(jnp.broadcast_to(row, (rows, rows)))[:, :1]
@@ -35,21 +36,25 @@
         sum(marks).astype(jnp.bfloat16),
         preferred_element_type=jnp.float32,
     )
-    slot_ids = lax.broadcasted_iota(jnp.int32, (rows, experts * sum(groups)), 1).astype(jnp.float32)
-    picked, share = 0.0, 0.0
-    for k in range(top_count):
-        rank = jnp.sum(before * marks[k], axis=1, keepdims=True)
-        slot, first, base = jnp.full((rows, 1), -1.0, jnp.float32), 0, 0
-        for g in groups:
-            inside = (rank >= first) & (rank < first + g)
-            slot = jnp.where(inside, base + names[k] * g + rank - first, slot)
-            first, base = first + g, base + g * experts
-        picked = picked + jnp.where(slot == slot_ids, 1.0, 0.0)
-        share = share + jnp.where(slot == slot_ids, shares[k], 0.0)
-    pick_ref[...] = jnp.transpose(picked).astype(jnp.bfloat16)
-    high = share.astype(jnp.bfloat16)
-    high_ref[...] = high
-    low_ref[...] = (share - high.astype(jnp.float32)).astype(jnp.bfloat16)
+    ranks = [jnp.sum(before * mark, axis=1, keepdims=True) for mark in marks]
+    slot_ids = lax.broadcasted_iota(jnp.int32, (rows, half * sum(groups)), 1).astype(jnp.float32)
+    for which, pick_ref, high_ref, low_ref in zip(halves, pick_refs, high_refs, low_refs):
+        start = jnp.asarray(which * half, jnp.int32).astype(jnp.float32)
+        picked, share = 0.0, 0.0
+        for k in range(top_count):
+            name, rank = names[k] - start, ranks[k]
+            here = (name >= 0.0) & (name < half)
+            slot, first, base = jnp.full((rows, 1), -1.0, jnp.float32), 0, 0
+            for g in groups:
+                inside = here & (rank >= first) & (rank < first + g)
+                slot = jnp.where(inside, base + name * g + rank - first, slot)
+                first, base = first + g, base + g * half
+            picked = picked + jnp.where(slot == slot_ids, 1.0, 0.0)
+            share = share + jnp.where(slot == slot_ids, shares[k], 0.0)
+        pick_ref[...] = jnp.transpose(picked).astype(jnp.bfloat16)
+        high = share.astype(jnp.bfloat16)
+        high_ref[...] = high
+        low_ref[...] = (share - high.astype(jnp.float32)).astype(jnp.bfloat16)
 
 
 def layer_kernel(sp, dp, count, *refs):
@@ -57,17 +62,20 @@
         q_hbm, k_hbm, v_hbm, weight_ref, resid_hbm, mixer_hbm, expert_hbm, routes_hbm, shares_hbm,
         gate_hbm, up_hbm, down_hbm, gain_hbm, out_ref,
     ) = refs[:14]
-    boxes = refs[14 : 14 + 4 * count]
+    boxes = refs[14 : 14 + 6 * count]
     sent, served = boxes[:count], boxes[count : 2 * count]
-    results, returned = boxes[2 * count : 3 * count], boxes[3 * count :]
+    results, returned = boxes[2 * count : 3 * count], boxes[3 * count : 4 * count]
+    lent, lent_back = boxes[4 * count : 5 * count], boxes[5 * count :]
     (
         raw, resid_ref, mixer_ref, expert_ref, gain_ref, routes_ref, shares_ref,
         stage, arrived, out_heads, in_heads, side_heads, flat, full, side_out, side_in,
         projected, tokens, stream_ref, pick_ref, high_ref, low_ref, gate_ref, up_ref, down_ref,
+        far_routes, far_shares, far_pick, far_high, far_low, dense, extra_ref,
         load_sem, q_send, q_recv, a_send, a_recv, pass_send, pass_recv, near_sem, far_send, far_recv,
         twin_send, twin_recv, side_send, side_recv, local_sem,
         send_sem, recv_sem, back_send, back_recv, keep_sem, fetch_sem,
-    ) = refs[14 + 4 * count :]
+        note_send, note_recv, dense_sem, partial_sem, lend_recv, lend_keep,
+    ) = refs[14 + 6 * count :]
     _, rows, heads, width = raw.shape
     local_heads = heads // sp
     depth, columns = weight_ref.shape
@@ -77,6 +85,15 @@
     ys = dp // 2
     own_y = lax.div(mate, 2)
     n, own = sp * dp, me * dp + mate
+    half, plane = n // 2, n // 4
+    level = lax.div(own, plane)
+    spot = lax.rem(own, plane)
+    my_half = lax.div(level, 2)
+    near_base, far_base = my_half * half, (1 - my_half) * half
+    local = own - near_base
+    partner = (3 - level) * plane + spot
+    inner = level == 1 + my_half
+    outer = level != 1 + my_half
 
     barrier = pltpu.get_barrier_semaphore()
 
@@ -168,11 +185,27 @@
         pltpu.make_async_copy(src, dst, fetch_sem.at[i])
         for i, (src, dst) in enumerate(((gate_hbm, gate_ref), (up_hbm, up_ref), (down_hbm, down_ref)))
     ]
-    for copy in fetches:
-        copy.start()
     loads[3].wait()
     loads[4].wait()
-    place_slots(rows, n, [box.shape[1] for box in sent], routes_ref, shares_ref, pick_ref, high_ref, low_ref)
+
+    def device(target):
+        return {"sp": lax.div(target, dp), "dp": lax.rem(target, dp)}
+
+    notes = [
+        remote(src, dst, note_send.at[i], note_recv.at[i], device(partner))
+        for i, (src, dst) in enumerate(((routes_ref, far_routes), (shares_ref, far_shares)))
+    ]
+    groups = [box.shape[1] for box in sent]
+
+    @pl.when(inner)
+    def _():
+        for note in notes:
+            note.start()
+
+    place_slots(
+        rows, n, groups, [0, 1], routes_ref, shares_ref,
+        *[[ref.at[i] for i in range(2)] for ref in (pick_ref, high_ref, low_ref)],
+    )
 
     block = rows * max(1, min(sp, 256 // rows))
     per = block // rows
@@ -198,7 +231,7 @@
             in_heads.at[h, source], side_heads.at[h, source], pass_send.at[h], pass_recv.at[h], {"sp": side}
         )
 
-    def attend_head(h):
+    def attend_head(h, between):
         def piece(t, index):
             return arrived[t, h, index * per : (index + 1) * per].reshape(block, width)
 
@@ -233,14 +266,19 @@
             out_heads[h, q_block * per : (q_block + 1) * per] = total.astype(jnp.bfloat16).reshape(
                 per, rows, width
             )
-
-    def send_answers(h):
-        def push(k, carry):
-            answer(h, lax.rem(me + k, sp)).start()
-            return carry
-
-        lax.fori_loop(1, sp, push, 0)
+            if q_block:
+                send_answers(h, q_block - 1)
+            if q_block == length // block // 2:
+                between()
+        send_answers(h, length // block - 1)
         keep_answer(h).start()
+
+    def send_answers(h, q_block):
+        for target in range(q_block * per, (q_block + 1) * per):
+
+            @pl.when(me != target)
+            def _():
+                answer(h, target).start()
 
     def keep_answer(h):
         return pltpu.make_async_copy(out_heads.at[h, me], in_heads.at[h, me], local_sem.at[3, h])
@@ -252,13 +290,7 @@
 
     for copy in keep_heads:
         copy.wait()
-    for h in range(local_heads):
-        await_bytes(arrived.at[:, h, others], q_recv.at[h])
-        attend_head(h)
-        send_answers(h)
-    for j in range(PIECES - 1):
-        pass_on(j)
-    for h in range(local_heads):
+    def follow_all(h):
         keep_answer(h).wait()
         hand_on(h, me).start()
 
@@ -269,7 +301,22 @@
             return carry
 
         lax.fori_loop(1, sp, follow, 0)
+
+    for h in range(local_heads):
+        await_bytes(arrived.at[:, h, others], q_recv.at[h])
+        attend_head(h, (lambda: follow_all(h - 1)) if h else (lambda: None))
+    for j in range(PIECES - 1):
+        pass_on(j)
+    follow_all(local_heads - 1)
     pass_on(PIECES - 1)
+    for copy in fetches:
+        copy.start()
+
+    @pl.when(inner)
+    def _():
+        for note in notes:
+            note.wait()
+        place_slots(rows, n, groups, [my_half], far_routes, far_shares, [far_pick], [far_high], [far_low])
 
     def fill(ref, first):
         for source in range(sp):
@@ -343,6 +390,10 @@
             projected[:, place_of(lax.rem(own_y + ys - d, ys) * 2 + 1 - parity, i)] = side_in[
                 d - 1, :, inner
             ].astype(jnp.float32)
+
+    def lend(i):
+        part = pl.ds(pl.multiple_of(i * 16, 16), 16)
+        return remote(tokens.at[part], dense.at[part], dense_sem.at[0], dense_sem.at[1], device(partner))
 
     @pl.loop(0, rows // 16)
     def _(i):
@@ -353,63 +404,121 @@
         stream_ref[part] = stream
         tokens[part] = normed_token_rows(stream.astype(jnp.float32), expert_ref[...]).astype(jnp.bfloat16)
 
+        @pl.when(inner & (i > 0))
+        def _():
+            lend(i - 1).start()
+
+    @pl.when(inner)
+    def _():
+        lend(rows // 16 - 1).start()
+
     features = projected.shape[1]
     tile = 512
 
-    def move(sources, targets, sends, recvs, a, target):
+    def each(number, turn, make, own_place):
+        def push(i, carry):
+            place = lax.rem(turn + i, number)
+
+            @pl.when(place != own_place)
+            def _():
+                make(place).start()
+
+            return carry
+
+        lax.fori_loop(0, number, push, 0)
+
+    def outward(a, target):
+        return remote(sent[a].at[target], served[a].at[own], send_sem.at[a], recv_sem.at[a], device(target))
+
+    def outward_lent(a, place):
         return remote(
-            sources[a].at[target], targets[a].at[own], sends.at[a], recvs.at[a],
-            {"sp": lax.div(target, dp), "dp": lax.rem(target, dp)},
-        )
-
-    def outward(a, target):
-        return move(sent, served, send_sem, recv_sem, a, target)
-
-    def homeward(a, target):
-        return move(results, returned, back_send, back_recv, a, target)
-
-    def start_all(make, a, first, number):
-        def push(i, carry):
-            target = first + lax.rem(lax.rem(own, number) + number // 2 + i, number)
-
-            @pl.when(target != own)
-            def _():
-                make(a, target).start()
-
-            return carry
-
-        lax.fori_loop(0, number, push, 0)
-
-    peers = pl.ds(0, n - 1)
-    half = n // 2
-    far_half = (1 - lax.div(own, half)) * half
+            lent[a].at[place], served[a].at[partner], send_sem.at[a], recv_sem.at[a], device(near_base + place)
+        )
+
+    def homeward(a, source):
+        return remote(results[a].at[source], returned[a].at[own], back_send.at[a], back_recv.at[a], device(source))
+
+    def homeward_lent(a, place):
+        return remote(
+            results[a].at[(2 - my_half) * plane + place], lent_back[a].at[local], back_send.at[a], lend_recv.at[a],
+            device((1 + my_half) * plane + place),
+        )
+
+    def choose(a, pick, source_ref, out, first):
+        row = half * sum(groups[:a])
+        wanted = pick[row : row + half * groups[a]]
+
+        @pl.loop(0, features // tile)
+        def _(i):
+            part = pl.ds(pl.multiple_of(i * tile, tile), tile)
+            out[a][pl.ds(first, half), :, part] = (
+                jnp.dot(wanted, source_ref[:, part], preferred_element_type=jnp.float32)
+                .astype(jnp.bfloat16)
+                .reshape(half, groups[a], tile)
+            )
+
     own_rows = [pltpu.make_async_copy(sent[a].at[own], served[a].at[own], keep_sem.at[a]) for a in range(count)]
     keeps = [
         pltpu.make_async_copy(results[a].at[own], returned[a].at[own], keep_sem.at[count + a])
         for a in range(count)
     ]
-    row = 0
+    lent_rows = [
+        pltpu.make_async_copy(lent[a].at[local], served[a].at[partner], lend_keep.at[a]) for a in range(count)
+    ]
+    lent_keeps = [
+        pltpu.make_async_copy(results[a].at[partner], lent_back[a].at[local], lend_keep.at[count + a])
+        for a in range(count)
+    ]
     for a in range(count):
-        many = sent[a].shape[1]
-        for first in (far_half, half - far_half):
-            wanted = pick_ref[pl.ds(pl.multiple_of(row + first * many, half * many), half * many)]
-
-            @pl.loop(0, features // tile)
-            def _(i):
-                part = pl.ds(pl.multiple_of(i * tile, tile), tile)
-                sent[a][pl.ds(first, half), :, part] = (
-                    jnp.dot(wanted, tokens[:, part], preferred_element_type=jnp.float32)
-                    .astype(jnp.bfloat16)
-                    .reshape(half, many, tile)
-                )
-
-            start_all(outward, a, first, half)
+
+        @pl.when(outer)
+        def _():
+            choose(a, pick_ref.at[1 - my_half], tokens, sent, far_base)
+            each(half, local + half // 2, lambda place: outward(a, far_base + place), -1)
+
+        choose(a, pick_ref.at[my_half], tokens, sent, near_base)
+        each(half, local + half // 2, lambda place: outward(a, near_base + place), local)
         own_rows[a].start()
-        row += n * many
+
+    @pl.when(inner)
+    def _():
+        await_bytes(dense, dense_sem.at[1])
+        for a in range(count):
+            choose(a, far_pick, dense, lent, 0)
+            each(half, local + half // 2, lambda place: outward_lent(a, place), local)
+            lent_rows[a].start()
+
+    def await_blocks(boxes, sems, a):
+        @pl.when(inner)
+        def _():
+            await_bytes(boxes[a].at[pl.ds(0, n - 2)], sems.at[a])
+
+        @pl.when(outer)
+        def _():
+            await_bytes(boxes[a].at[pl.ds(0, n - 1)], sems.at[a])
+
+    def give_lent(a):
+        each(plane, spot + plane // 2, lambda place: homeward_lent(a, place), jnp.where(inner, spot, -1))
+
+        @pl.when(inner)
+        def _():
+            lent_keeps[a].start()
+
+    def give_far(a):
+        each(plane, spot + plane // 2, lambda place: homeward(a, 3 * (1 - my_half) * plane + place), -1)
+
+    def give_near(a):
+        each(half, local + half // 2, lambda place: homeward(a, near_base + place), local)
+        keeps[a].start()
 
     for a in range(count):
         own_rows[a].wait()
-        await_bytes(served[a].at[peers], recv_sem.at[a])
+
+        @pl.when(inner)
+        def _():
+            lent_rows[a].wait()
+
+        await_blocks(served, recv_sem, a)
         if a == 0:
             for copy in fetches:
                 copy.wait()
@@ -425,31 +534,92 @@
                 .astype(jnp.bfloat16)
                 .reshape(n, many, tile)
             )
-        start_all(homeward, a, far_half, half)
-        start_all(homeward, a, half - far_half, half)
-        keeps[a].start()
-
-    row = 0
+        give_lent(a)
+
+        @pl.when(inner)
+        def _():
+            give_far(a)
+
     for a in range(count):
-        keeps[a].wait()
-        await_bytes(returned[a].at[peers], back_recv.at[a])
-        many = returned[a].shape[1]
-        columns_of = slice(row, row + n * many)
+
+        @pl.when(outer)
+        def _():
+            give_far(a)
+
+        give_near(a)
+
+    def gather(box, first, high, low, a, part):
+        columns_of = slice(half * sum(groups[:a]), half * sum(groups[: a + 1]))
+        block = box[a][pl.ds(first, half), :, part].reshape(half * groups[a], tile)
+        return jnp.dot(high[:, columns_of], block, preferred_element_type=jnp.float32) + jnp.dot(
+            low[:, columns_of], block, preferred_element_type=jnp.float32
+        )
+
+    def settle_up(i):
+        part = pl.ds(pl.multiple_of(i * tile, tile), tile)
+        return remote(
+            dense.at[:, part], extra_ref.at[:, part], partial_sem.at[0], partial_sem.at[1], device(partner)
+        )
+
+    @pl.when(inner)
+    def _():
+        for a in range(count):
+            lent_keeps[a].wait()
+            await_bytes(lent_back[a].at[pl.ds(0, half - 1)], lend_recv.at[a])
 
         @pl.loop(0, features // tile)
         def _(i):
             part = pl.ds(pl.multiple_of(i * tile, tile), tile)
-            block = returned[a][:, :, part].reshape(n * many, tile)
-            total = jnp.dot(high_ref[:, columns_of], block, preferred_element_type=jnp.float32) + jnp.dot(
-                low_ref[:, columns_of], block, preferred_element_type=jnp.float32
-            )
+            dense[:, part] = sum(
+                gather(lent_back, 0, far_high, far_low, a, part) for a in range(count)
+            ).astype(jnp.bfloat16)
+
+            @pl.when(i > 0)
+            def _():
+                settle_up(i - 1).start()
+
+        settle_up(features // tile - 1).start()
+
+    for a in range(count):
+        keeps[a].wait()
+
+        @pl.when(inner)
+        def _():
+            await_bytes(returned[a].at[pl.ds(0, half - 1)], back_recv.at[a])
+
+        @pl.when(outer)
+        def _():
+            await_bytes(returned[a].at[pl.ds(0, n - 1)], back_recv.at[a])
+
+        @pl.loop(0, features // tile)
+        def _(i):
+            part = pl.ds(pl.multiple_of(i * tile, tile), tile)
+            total = gather(returned, near_base, high_ref.at[my_half], low_ref.at[my_half], a, part)
             projected[:, part] = total if a == 0 else projected[:, part] + total
 
-        row += n * many
+        @pl.when(outer)
+        def _():
+            @pl.loop(0, features // tile)
+            def _(i):
+                part = pl.ds(pl.multiple_of(i * tile, tile), tile)
+                projected[:, part] += gather(
+                    returned, far_base, high_ref.at[1 - my_half], low_ref.at[1 - my_half], a, part
+                )
 
     for a in range(count):
-        await_bytes(sent[a].at[peers], send_sem.at[a])
-        await_bytes(results[a].at[peers], back_send.at[a])
+        await_blocks(sent, send_sem, a)
+        await_blocks(results, back_send, a)
+
+    @pl.when(inner)
+    def _():
+        await_bytes(tokens, dense_sem.at[0])
+        await_bytes(dense, partial_sem.at[0])
+        await_bytes(extra_ref, partial_sem.at[1])
+
+        @pl.loop(0, rows // 16)
+        def _(i):
+            part = pl.ds(pl.multiple_of(i * 16, 16), 16)
+            projected[part] += extra_ref[part].astype(jnp.float32)
 
     @pl.loop(0, rows // 16)
     def _(i):
@@ -469,7 +639,7 @@
     features = residual.shape[1]
     local_heads = heads // sp
     extra = max(dp // 2 - 1, 1)
-    slots = n * sum(groups)
+    slots = n // 2 * sum(groups)
     anywhere = pl.BlockSpec(memory_space=pl.ANY)
     dma = pltpu.SemaphoreType.DMA
     bf16, f32 = jnp.bfloat16, jnp.float32
@@ -479,6 +649,7 @@
         in_specs=[anywhere] * 13,
         out_specs=pl.BlockSpec(memory_space=pltpu.VMEM),
         scratch_shapes=[pltpu.VMEM((n, g, features), bf16) for _ in range(4) for g in groups]
+        + [pltpu.VMEM((n // 2, g, features), bf16) for _ in range(2) for g in groups]
         + [
             pltpu.VMEM((3, rows, heads, width), bf16),
             pltpu.VMEM((rows, features), bf16),
@@ -499,12 +670,19 @@
             pltpu.VMEM((rows, features), f32),
             pltpu.VMEM((rows, features), bf16),
             pltpu.VMEM((rows, features), bf16),
+            pltpu.VMEM((2, slots, rows), bf16),
+            pltpu.VMEM((2, rows, slots), bf16),
+            pltpu.VMEM((2, rows, slots), bf16),
+            pltpu.VMEM(gate.shape, bf16),
+            pltpu.VMEM(up.shape, bf16),
+            pltpu.VMEM(down.shape, bf16),
+            pltpu.VMEM(routes.shape, jnp.int32),
+            pltpu.VMEM(shares.shape, f32),
             pltpu.VMEM((slots, rows), bf16),
             pltpu.VMEM((rows, slots), bf16),
             pltpu.VMEM((rows, slots), bf16),
-            pltpu.VMEM(gate.shape, bf16),
-            pltpu.VMEM(up.shape, bf16),
-            pltpu.VMEM(down.shape, bf16),
+            pltpu.VMEM((rows, features), bf16),
+            pltpu.VMEM((rows, features), bf16),
             dma((10,)),
             dma((local_heads,)),
             dma((local_heads,)),
@@ -526,6 +704,12 @@
             dma((len(groups),)),
             dma((2 * len(groups),)),
             dma((3,)),
+            dma((2,)),
+            dma((2,)),
+            dma((2,)),
+            dma((2,)),
+            dma((len(groups),)),
+            dma((2 * len(groups),)),
         ],
         compiler_params=pltpu.CompilerParams(
             collective_id=0, has_side_effects=True, vmem_limit_bytes=VMEM_LIMIT

time: 220 us -> 224 us (1.018)
  Pallas kernels: 217 us -> 221 us
    pallas_call x1, Pallas kernels: 217 us -> 221 us  [layer(): pl.pallas_call(functools.partial(layer_kernel, sp, dp, len(groups)), out_...]
where the time goes in v5:
time: 224 us; the launch traced here: 222 us
  Pallas kernels  221 us (99%)
    pallas_call x1, Pallas kernels, layer(): pl.pallas_call(functools.partial(layer_kernel, sp, dp, len(groups)), out_...  221 us

profile of v5, /device:TPU:16, one launch (start us, length us, event | category | flops | bytes accessed | tf_op | source)
XLA Modules:
  0.0 221.5 jit_solution(8378562747542527196)
XLA Ops:
  0.0 220.5 %shard_map.127 = bf16[128,4096]{1,0:T(8,128)(2,1)S(1)} custom-call(bf16[128,16,128]{2,1,0:T(8,128)(2,1)} %bitcast.22, bf16[128,16,128]{2,1,0:T(8,128)(2,1)} %bitcast.23, bf16[128,16,128]{2,1,0:T(8,128)(2,1)} %bitcast.24, bf16[2048,1024]{1,0:T(8,128)(2,1)} %refs_3_.1, bf16[128,4096]{1,0:T(8,128)(2,1)} %bitcast.21, f32[1,4096]{1,0:T(1,128)} %bitcast.25, ...), custom_call_target="tpu_custom_call" | custom-call | tf_op jit(solution)/shard_map/pallas_call | solution.py:646
  220.6 1.0 copy.15

commit v6 on v5

--- a/solution.py
+++ b/solution.py
@@ -74,7 +74,7 @@
         load_sem, q_send, q_recv, a_send, a_recv, pass_send, pass_recv, near_sem, far_send, far_recv,
         twin_send, twin_recv, side_send, side_recv, local_sem,
         send_sem, recv_sem, back_send, back_recv, keep_sem, fetch_sem,
-        note_send, note_recv, dense_sem, partial_sem, lend_recv, lend_keep,
+        note_send, note_recv, dense_sem, partial_sem, lend_recv, lend_keep, turn_sem,
     ) = refs[14 + 6 * count :]
     _, rows, heads, width = raw.shape
     local_heads = heads // sp
@@ -470,18 +470,29 @@
         for a in range(count)
     ]
     for a in range(count):
-
-        @pl.when(outer)
-        def _():
-            choose(a, pick_ref.at[1 - my_half], tokens, sent, far_base)
-            each(half, local + half // 2, lambda place: outward(a, far_base + place), -1)
-
         choose(a, pick_ref.at[my_half], tokens, sent, near_base)
         each(half, local + half // 2, lambda place: outward(a, near_base + place), local)
         own_rows[a].start()
 
+    @pl.when(outer)
+    def _():
+        for a in range(count):
+            choose(a, pick_ref.at[1 - my_half], tokens, sent, far_base)
+        pl.semaphore_wait(turn_sem, plane)
+        for a in range(count):
+            each(half, local + half // 2, lambda place: outward(a, far_base + place), -1)
+
     @pl.when(inner)
     def _():
+        await_bytes(tokens, dense_sem.at[0])
+
+        def release(i, carry):
+            pl.semaphore_signal(
+                turn_sem, inc=1, device_id=device(3 * my_half * plane + i), device_id_type=MESH
+            )
+            return carry
+
+        lax.fori_loop(0, plane, release, 0)
         await_bytes(dense, dense_sem.at[1])
         for a in range(count):
             choose(a, far_pick, dense, lent, 0)
@@ -612,7 +623,6 @@
 
     @pl.when(inner)
     def _():
-        await_bytes(tokens, dense_sem.at[0])
         await_bytes(dense, partial_sem.at[0])
         await_bytes(extra_ref, partial_sem.at[1])
 
@@ -710,6 +720,7 @@
             dma((2,)),
             dma((len(groups),)),
             dma((2 * len(groups),)),
+            pltpu.SemaphoreType.REGULAR,
         ],
         compiler_params=pltpu.CompilerParams(
             collective_id=0, has_side_effects=True, vmem_limit_bytes=VMEM_LIMIT

time: 224 us -> 190 us (0.85)
  Pallas kernels: 221 us -> 188 us
    pallas_call x1, Pallas kernels: 221 us -> 188 us  [layer(): pl.pallas_call(functools.partial(layer_kernel, sp, dp, len(groups)), out_...]
where the time goes in v6:
time: 190 us; the launch traced here: 189 us
  Pallas kernels  188 us (99%)
    pallas_call x1, Pallas kernels, layer(): pl.pallas_call(functools.partial(layer_kernel, sp, dp, len(groups)), out_...  188 us

profile of v6, /device:TPU:16, one launch (start us, length us, event | category | flops | bytes accessed | tf_op | source)
XLA Modules:
  0.0 188.6 jit_solution(10971477214147337713)
XLA Ops:
  0.0 187.6 %shard_map.127 = bf16[128,4096]{1,0:T(8,128)(2,1)S(1)} custom-call(bf16[128,16,128]{2,1,0:T(8,128)(2,1)} %bitcast.22, bf16[128,16,128]{2,1,0:T(8,128)(2,1)} %bitcast.23, bf16[128,16,128]{2,1,0:T(8,128)(2,1)} %bitcast.24, bf16[2048,1024]{1,0:T(8,128)(2,1)} %refs_3_.1, bf16[128,4096]{1,0:T(8,128)(2,1)} %bitcast.21, f32[1,4096]{1,0:T(1,128)} %bitcast.25, ...), custom_call_target="tpu_custom_call" | custom-call | tf_op jit(solution)/shard_map/pallas_call | solution.py:656
  187.6 1.0 copy.15

commit v7 on v6

--- a/solution.py
+++ b/solution.py
@@ -67,14 +67,15 @@
     results, returned = boxes[2 * count : 3 * count], boxes[3 * count : 4 * count]
     lent, lent_back = boxes[4 * count : 5 * count], boxes[5 * count :]
     (
-        raw, resid_ref, mixer_ref, expert_ref, gain_ref, routes_ref, shares_ref,
-        stage, arrived, out_heads, in_heads, side_heads, flat, full, side_out, side_in,
-        projected, tokens, stream_ref, pick_ref, high_ref, low_ref, gate_ref, up_ref, down_ref,
+        raw, stream_ref, mixer_ref, expert_ref, gain_ref, routes_ref, shares_ref,
+        stage, arrived, out_heads, in_heads, side_heads, flat, full, side_out, side_in, peer_heads, peer_out, peer_in,
+        projected, tokens, pick_ref, high_ref, low_ref, gate_ref, up_ref, down_ref,
         far_routes, far_shares, far_pick, far_high, far_low, dense, extra_ref,
         load_sem, q_send, q_recv, a_send, a_recv, pass_send, pass_recv, near_sem, far_send, far_recv,
         twin_send, twin_recv, side_send, side_recv, local_sem,
         send_sem, recv_sem, back_send, back_recv, keep_sem, fetch_sem,
         note_send, note_recv, dense_sem, partial_sem, lend_recv, lend_keep, turn_sem,
+        ask_send, ask_recv, peer_send, peer_recv,
     ) = refs[14 + 6 * count :]
     _, rows, heads, width = raw.shape
     local_heads = heads // sp
@@ -107,7 +108,7 @@
     lax.fori_loop(1, n, greet, 0)
     pairs = [
         (q_hbm, raw.at[0]), (k_hbm, raw.at[1]), (v_hbm, raw.at[2]), (routes_hbm, routes_ref),
-        (shares_hbm, shares_ref), (weight_ref, full.at[core]), (resid_hbm, resid_ref), (mixer_hbm, mixer_ref),
+        (shares_hbm, shares_ref), (weight_ref, full.at[core]), (resid_hbm, stream_ref), (mixer_hbm, mixer_ref),
         (expert_hbm, expert_ref), (gain_hbm, gain_ref),
     ]
     loads = [pltpu.make_async_copy(src, dst, load_sem.at[i]) for i, (src, dst) in enumerate(pairs)]
@@ -207,6 +208,7 @@
         *[[ref.at[i] for i in range(2)] for ref in (pick_ref, high_ref, low_ref)],
     )
 
+    part_rows = rows // 2
     block = rows * max(1, min(sp, 256 // rows))
     per = block // rows
     length = sp * rows
@@ -227,9 +229,15 @@
         )
 
     def hand_on(h, source):
-        return remote(
-            in_heads.at[h, source], side_heads.at[h, source], pass_send.at[h], pass_recv.at[h], {"sp": side}
-        )
+        remote(
+            in_heads.at[h, source, :part_rows], side_heads.at[h, source], pass_send.at[h], pass_recv.at[h],
+            {"sp": side},
+        ).start()
+        for d in range(1, ys):
+            remote(
+                in_heads.at[h, source, part_rows:], peer_heads.at[d - 1, h, source], ask_send.at[d - 1, h],
+                ask_recv.at[d - 1, h], {"dp": lax.rem(own_y + ys - d, ys) * 2 + core},
+            ).start()
 
     def attend_head(h, between):
         def piece(t, index):
@@ -292,12 +300,16 @@
         copy.wait()
     def follow_all(h):
         keep_answer(h).wait()
-        hand_on(h, me).start()
+        hand_on(h, me)
 
         def follow(k, carry):
-            source = lax.rem(me + k, sp)
-            expect(h, source).wait_recv()
-            hand_on(h, source).start()
+            for source in (me + k, me - k):
+
+                @pl.when((source >= 0) & (source < sp))
+                def _():
+                    expect(h, source).wait_recv()
+                    hand_on(h, source)
+
             return carry
 
         lax.fori_loop(1, sp, follow, 0)
@@ -322,12 +334,13 @@
         for source in range(sp):
             for h in range(local_heads):
                 place = (source * local_heads + h) * width
-                flat[first : first + rows, place : place + width] = ref[h, source]
-
-    fill(in_heads, 0)
+                block = ref[h, source]
+                flat[first : first + block.shape[0], place : place + width] = block
+
+    fill(in_heads, part_rows)
     for h in range(local_heads):
         await_bytes(side_heads.at[h], pass_recv.at[h])
-    fill(side_heads, rows)
+    fill(side_heads, 0)
     for d in range(1, ys):
         for j in range(PIECES):
             to_twin(d, j).wait()
@@ -335,36 +348,71 @@
     tile = min(columns, 512)
     many = columns // tile
 
-    def split(i):
-        return lax.div(i, many), pl.ds(pl.multiple_of(lax.rem(i, many) * tile, tile), tile)
+    def inner_part(i):
+        return pl.ds(pl.multiple_of(i * tile, tile), tile)
 
     def place_of(slice_index, i):
-        return pl.ds(pl.multiple_of((slice_index * many + lax.rem(i, many)) * tile, tile), tile)
-
-    def hand_back(d):
+        return pl.ds(pl.multiple_of((slice_index * many + i) * tile, tile), tile)
+
+    def origin(d):
+        return lax.rem(own_y + ys - d, ys) * 2
+
+    def hand_back(d, inner):
         return remote(
-            side_out.at[d - 1], side_in.at[d - 1], side_send.at[d - 1], side_recv.at[d - 1], {"sp": side}
+            side_out.at[d - 1, :, inner], side_in.at[d - 1, :, inner], side_send.at[d - 1], side_recv.at[d - 1],
+            {"sp": side},
+        )
+
+    def reply(d, inner):
+        return remote(
+            peer_out.at[d - 1, :, inner], peer_in.at[d - 1, :, inner], peer_send.at[d - 1], peer_recv.at[d - 1],
+            {"dp": lax.rem(own_y + d, ys) * 2 + core},
         )
 
     for d in range(1, ys):
 
         @pl.loop(0, many)
         def _(i):
-            _, inner = split(i)
-            both = jnp.dot(flat[...], full[1 + d, :, inner], preferred_element_type=jnp.float32)
-            projected[:, place_of(lax.rem(own_y + ys - d, ys) * 2 + parity, i)] = both[:rows]
-            side_out[d - 1, :, inner] = both[rows:].astype(jnp.bfloat16)
-
-        hand_back(d).start()
-
+            inner = inner_part(i)
+            both = jnp.dot(flat[: part_rows + rows], full[1 + d, :, inner], preferred_element_type=jnp.float32)
+            projected[:, place_of(origin(d) + parity, i)] = both[part_rows:]
+            side_out[d - 1, :, inner] = both[:part_rows].astype(jnp.bfloat16)
+
+            @pl.when(i > 0)
+            def _():
+                hand_back(d, inner_part(i - 1)).start()
+
+        hand_back(d, pl.ds((many - 1) * tile, tile)).start()
+
+    for d in range(1, ys):
+        for h in range(local_heads):
+            await_bytes(peer_heads.at[d - 1, h], ask_recv.at[d - 1, h])
+        fill(peer_heads.at[d - 1], part_rows + rows + (d - 1) * part_rows)
     loads[5].wait()
     near.wait()
 
-    @pl.loop(0, 2 * many)
+    @pl.loop(0, many)
     def _(i):
-        which, inner = split(i)
-        projected[:, place_of(own_y * 2 + which, i)] = jnp.dot(
-            flat[:rows], full[which, :, inner], preferred_element_type=jnp.float32
+        inner = inner_part(i)
+        both = jnp.dot(flat[part_rows:], full[1 - parity, :, inner], preferred_element_type=jnp.float32)
+        projected[:, place_of(own_y * 2 + 1 - parity, i)] = both[:rows]
+        for d in range(1, ys):
+            peer_out[d - 1, :, inner] = both[
+                rows + (d - 1) * part_rows : rows + d * part_rows
+            ].astype(jnp.bfloat16)
+
+        @pl.when(i > 0)
+        def _():
+            for d in range(1, ys):
+                reply(d, inner_part(i - 1)).start()
+
+    for d in range(1, ys):
+        reply(d, pl.ds((many - 1) * tile, tile)).start()
+
+    @pl.loop(0, many)
+    def _(i):
+        projected[:, place_of(own_y * 2 + parity, i)] = jnp.dot(
+            flat[part_rows : part_rows + rows], full[parity, :, inner_part(i)], preferred_element_type=jnp.float32
         )
 
     for load in loads[6:]:
@@ -372,7 +420,9 @@
     for h in range(local_heads):
         await_bytes(stage.at[:, others], q_send.at[h])
         await_bytes(out_heads.at[h, others], a_send.at[h])
-        await_bytes(in_heads.at[h], pass_send.at[h])
+        await_bytes(side_heads.at[h], pass_send.at[h])
+        for d in range(1, ys):
+            await_bytes(peer_heads.at[d - 1, h], ask_send.at[d - 1, h])
 
     @pl.when(core == parity)
     def _():
@@ -382,14 +432,16 @@
                     far(d, owner, j).wait_send()
 
     for d in range(1, ys):
-        hand_back(d).wait()
+        await_bytes(side_in.at[d - 1], side_recv.at[d - 1])
+        await_bytes(side_out.at[d - 1], side_send.at[d - 1])
+        await_bytes(peer_in.at[d - 1], peer_recv.at[d - 1])
+        await_bytes(peer_out.at[d - 1], peer_send.at[d - 1])
 
         @pl.loop(0, many)
         def _(i):
-            _, inner = split(i)
-            projected[:, place_of(lax.rem(own_y + ys - d, ys) * 2 + 1 - parity, i)] = side_in[
-                d - 1, :, inner
-            ].astype(jnp.float32)
+            outer_part = place_of(origin(d) + 1 - parity, i)
+            projected[:part_rows, outer_part] = side_in[d - 1, :, inner_part(i)].astype(jnp.float32)
+            projected[part_rows:, outer_part] = peer_in[d - 1, :, inner_part(i)].astype(jnp.float32)
 
     def lend(i):
         part = pl.ds(pl.multiple_of(i * 16, 16), 16)
@@ -399,7 +451,7 @@
     def _(i):
         part = pl.ds(pl.multiple_of(i * 16, 16), 16)
         stream = (
-            resid_ref[part].astype(jnp.float32) + normed_token_rows(projected[part], mixer_ref[...])
+            stream_ref[part].astype(jnp.float32) + normed_token_rows(projected[part], mixer_ref[...])
         ).astype(jnp.bfloat16)
         stream_ref[part] = stream
         tokens[part] = normed_token_rows(stream.astype(jnp.float32), expert_ref[...]).astype(jnp.bfloat16)
@@ -621,22 +673,24 @@
         await_blocks(sent, send_sem, a)
         await_blocks(results, back_send, a)
 
-    @pl.when(inner)
-    def _():
-        await_bytes(dense, partial_sem.at[0])
-        await_bytes(extra_ref, partial_sem.at[1])
-
+    def finish(combined):
         @pl.loop(0, rows // 16)
         def _(i):
             part = pl.ds(pl.multiple_of(i * 16, 16), 16)
-            projected[part] += extra_ref[part].astype(jnp.float32)
-
-    @pl.loop(0, rows // 16)
-    def _(i):
-        part = pl.ds(pl.multiple_of(i * 16, 16), 16)
-        out_ref[part] = (
-            stream_ref[part].astype(jnp.float32) + normed_token_rows(projected[part], gain_ref[...])
-        ).astype(jnp.bfloat16)
+            out_ref[part] = (
+                stream_ref[part].astype(jnp.float32) + normed_token_rows(combined(part), gain_ref[...])
+            ).astype(jnp.bfloat16)
+
+    @pl.when(inner)
+    def _():
+        await_bytes(dense, partial_sem.at[0])
+        await_bytes(extra_ref, partial_sem.at[1])
+
+        finish(lambda part: projected[part] + extra_ref[part].astype(jnp.float32))
+
+    @pl.when(outer)
+    def _():
+        finish(lambda part: projected[part])
 
 
 def layer(
@@ -672,13 +726,15 @@
             pltpu.VMEM((3, local_heads, sp, rows, width), bf16),
             pltpu.VMEM((local_heads, sp, rows, width), bf16),
             pltpu.VMEM((local_heads, sp, rows, width), bf16),
-            pltpu.VMEM((local_heads, sp, rows, width), bf16),
-            pltpu.VMEM((2 * rows, depth), bf16),
+            pltpu.VMEM((local_heads, sp, rows // 2, width), bf16),
+            pltpu.VMEM(((3 + extra) * (rows // 2), depth), bf16),
             pltpu.VMEM((2 + extra, depth, columns), bf16),
-            pltpu.VMEM((extra, rows, columns), bf16),
-            pltpu.VMEM((extra, rows, columns), bf16),
+            pltpu.VMEM((extra, rows // 2, columns), bf16),
+            pltpu.VMEM((extra, rows // 2, columns), bf16),
+            pltpu.VMEM((extra, local_heads, sp, rows // 2, width), bf16),
+            pltpu.VMEM((extra, rows // 2, columns), bf16),
+            pltpu.VMEM((extra, rows // 2, columns), bf16),
             pltpu.VMEM((rows, features), f32),
-            pltpu.VMEM((rows, features), bf16),
             pltpu.VMEM((rows, features), bf16),
             pltpu.VMEM((2, slots, rows), bf16),
             pltpu.VMEM((2, rows, slots), bf16),
@@ -721,6 +777,10 @@
             dma((len(groups),)),
             dma((2 * len(groups),)),
             pltpu.SemaphoreType.REGULAR,
+            dma((extra, local_heads)),
+            dma((extra, local_heads)),
+            dma((extra,)),
+            dma((extra,)),
         ],
         compiler_params=pltpu.CompilerParams(
             collective_id=0, has_side_effects=True, vmem_limit_bytes=VMEM_LIMIT

time: 190 us -> 185 us (0.974)
  Pallas kernels: 188 us -> 183 us
    pallas_call x1, Pallas kernels: 188 us -> 183 us  [layer(): pl.pallas_call(functools.partial(layer_kernel, sp, dp, len(groups)), out_...]
where the time goes in v7:
time: 185 us; the launch traced here: 184 us
  Pallas kernels  183 us (99%)
    pallas_call x1, Pallas kernels, layer(): pl.pallas_call(functools.partial(layer_kernel, sp, dp, len(groups)), out_...  183 us

profile of v7, /device:TPU:16, one launch (start us, length us, event | category | flops | bytes accessed | tf_op | source)
XLA Modules:
  0.0 183.7 jit_solution(8421628586802036675)
XLA Ops:
  0.0 182.7 %shard_map.127 = bf16[128,4096]{1,0:T(8,128)(2,1)S(1)} custom-call(bf16[128,16,128]{2,1,0:T(8,128)(2,1)} %bitcast.22, bf16[128,16,128]{2,1,0:T(8,128)(2,1)} %bitcast.23, bf16[128,16,128]{2,1,0:T(8,128)(2,1)} %bitcast.24, bf16[2048,1024]{1,0:T(8,128)(2,1)} %refs_3_.1, bf16[128,4096]{1,0:T(8,128)(2,1)} %bitcast.21, f32[1,4096]{1,0:T(1,128)} %bitcast.25, ...), custom_call_target="tpu_custom_call" | custom-call | tf_op jit(solution)/shard_map/pallas_call | solution.py:710
  182.7 1.0 copy.15

commit v8 on v7

--- a/solution.py
+++ b/solution.py
@@ -19,7 +19,7 @@
 PIECES = 2
 
 
-def place_slots(rows, experts, groups, halves, routes_ref, shares_ref, pick_refs, high_refs, low_refs):
+def place_slots(rows, experts, groups, halves, routes_ref, shares_ref, pick_refs, part_refs):
     top_count = routes_ref.shape[0]
     half = experts // 2
 
@@ -38,7 +38,7 @@
     )
     ranks = [jnp.sum(before * mark, axis=1, keepdims=True) for mark in marks]
     slot_ids = lax.broadcasted_iota(jnp.int32, (rows, half * sum(groups)), 1).astype(jnp.float32)
-    for which, pick_ref, high_ref, low_ref in zip(halves, pick_refs, high_refs, low_refs):
+    for which, pick_ref, part_ref in zip(halves, pick_refs, part_refs):
         start = jnp.asarray(which * half, jnp.int32).astype(jnp.float32)
         picked, share = 0.0, 0.0
         for k in range(top_count):
@@ -53,8 +53,8 @@
             share = share + jnp.where(slot == slot_ids, shares[k], 0.0)
         pick_ref[...] = jnp.transpose(picked).astype(jnp.bfloat16)
         high = share.astype(jnp.bfloat16)
-        high_ref[...] = high
-        low_ref[...] = (share - high.astype(jnp.float32)).astype(jnp.bfloat16)
+        part_ref[:rows] = high
+        part_ref[rows:] = (share - high.astype(jnp.float32)).astype(jnp.bfloat16)
 
 
 def layer_kernel(sp, dp, count, *refs):
@@ -69,8 +69,8 @@
     (
         raw, stream_ref, mixer_ref, expert_ref, gain_ref, routes_ref, shares_ref,
         stage, arrived, out_heads, in_heads, side_heads, flat, full, side_out, side_in, peer_heads, peer_out, peer_in,
-        projected, tokens, pick_ref, high_ref, low_ref, gate_ref, up_ref, down_ref,
-        far_routes, far_shares, far_pick, far_high, far_low, dense, extra_ref,
+        projected, tokens, pick_ref, part_ref, gate_ref, up_ref, down_ref,
+        far_routes, far_shares, far_pick, far_part, dense, extra_ref,
         load_sem, q_send, q_recv, a_send, a_recv, pass_send, pass_recv, near_sem, far_send, far_recv,
         twin_send, twin_recv, side_send, side_recv, local_sem,
         send_sem, recv_sem, back_send, back_recv, keep_sem, fetch_sem,
@@ -205,7 +205,7 @@
 
     place_slots(
         rows, n, groups, [0, 1], routes_ref, shares_ref,
-        *[[ref.at[i] for i in range(2)] for ref in (pick_ref, high_ref, low_ref)],
+        *[[ref.at[i] for i in range(2)] for ref in (pick_ref, part_ref)],
     )
 
     part_rows = rows // 2
@@ -239,11 +239,14 @@
                 ask_recv.at[d - 1, h], {"dp": lax.rem(own_y + ys - d, ys) * 2 + core},
             ).start()
 
+    ends = length // block
+    turns = [ends - 1 - i // 2 if i % 2 == 0 else i // 2 for i in range(ends)]
+
     def attend_head(h, between):
         def piece(t, index):
             return arrived[t, h, index * per : (index + 1) * per].reshape(block, width)
 
-        for q_block in range(length // block):
+        for step, q_block in enumerate(turns):
             query = piece(0, q_block)
             total = jnp.zeros((block, width), jnp.float32)
             later = jnp.zeros((block, 1), jnp.float32)
@@ -274,11 +277,11 @@
             out_heads[h, q_block * per : (q_block + 1) * per] = total.astype(jnp.bfloat16).reshape(
                 per, rows, width
             )
-            if q_block:
-                send_answers(h, q_block - 1)
-            if q_block == length // block // 2:
+            if step:
+                send_answers(h, turns[step - 1])
+            if step == len(turns) // 2:
                 between()
-        send_answers(h, length // block - 1)
+        send_answers(h, turns[-1])
         keep_answer(h).start()
 
     def send_answers(h, q_block):
@@ -328,7 +331,7 @@
     def _():
         for note in notes:
             note.wait()
-        place_slots(rows, n, groups, [my_half], far_routes, far_shares, [far_pick], [far_high], [far_low])
+        place_slots(rows, n, groups, [my_half], far_routes, far_shares, [far_pick], [far_part])
 
     def fill(ref, first):
         for source in range(sp):
@@ -611,17 +614,19 @@
 
         give_near(a)
 
-    def gather(box, first, high, low, a, part):
+    def gather(box, first, parts, a, part):
         columns_of = slice(half * sum(groups[:a]), half * sum(groups[: a + 1]))
         block = box[a][pl.ds(first, half), :, part].reshape(half * groups[a], tile)
-        return jnp.dot(high[:, columns_of], block, preferred_element_type=jnp.float32) + jnp.dot(
-            low[:, columns_of], block, preferred_element_type=jnp.float32
-        )
-
-    def settle_up(i):
+        both = jnp.dot(parts[:, columns_of], block, preferred_element_type=jnp.float32)
+        return both[:rows] + both[rows:]
+
+    pieces = [slice(0, part_rows), slice(part_rows, rows)]
+
+    def settle_up(r, i):
         part = pl.ds(pl.multiple_of(i * tile, tile), tile)
         return remote(
-            dense.at[:, part], extra_ref.at[:, part], partial_sem.at[0], partial_sem.at[1], device(partner)
+            dense.at[pieces[r], part], extra_ref.at[pieces[r], part], partial_sem.at[0], partial_sem.at[1 + r],
+            device(partner),
         )
 
     @pl.when(inner)
@@ -634,14 +639,18 @@
         def _(i):
             part = pl.ds(pl.multiple_of(i * tile, tile), tile)
             dense[:, part] = sum(
-                gather(lent_back, 0, far_high, far_low, a, part) for a in range(count)
+                gather(lent_back, 0, far_part, a, part) for a in range(count)
             ).astype(jnp.bfloat16)
 
             @pl.when(i > 0)
             def _():
-                settle_up(i - 1).start()
-
-        settle_up(features // tile - 1).start()
+                settle_up(0, i - 1).start()
+
+        settle_up(0, features // tile - 1).start()
+
+        @pl.loop(0, features // tile)
+        def _(i):
+            settle_up(1, i).start()
 
     for a in range(count):
         keeps[a].wait()
@@ -654,27 +663,27 @@
         def _():
             await_bytes(returned[a].at[pl.ds(0, n - 1)], back_recv.at[a])
 
-        @pl.loop(0, features // tile)
-        def _(i):
-            part = pl.ds(pl.multiple_of(i * tile, tile), tile)
-            total = gather(returned, near_base, high_ref.at[my_half], low_ref.at[my_half], a, part)
-            projected[:, part] = total if a == 0 else projected[:, part] + total
-
-        @pl.when(outer)
-        def _():
+        def add_up(bases):
             @pl.loop(0, features // tile)
             def _(i):
                 part = pl.ds(pl.multiple_of(i * tile, tile), tile)
-                projected[:, part] += gather(
-                    returned, far_base, high_ref.at[1 - my_half], low_ref.at[1 - my_half], a, part
-                )
+                total = sum(gather(returned, first, part_ref.at[which], a, part) for first, which in bases)
+                projected[:, part] = total if a == 0 else projected[:, part] + total
+
+        @pl.when(inner)
+        def _():
+            add_up([(near_base, my_half)])
+
+        @pl.when(outer)
+        def _():
+            add_up([(near_base, my_half), (far_base, 1 - my_half)])
 
     for a in range(count):
         await_blocks(sent, send_sem, a)
         await_blocks(results, back_send, a)
 
-    def finish(combined):
-        @pl.loop(0, rows // 16)
+    def finish(combined, piece):
+        @pl.loop(piece.start // 16, piece.stop // 16)
         def _(i):
             part = pl.ds(pl.multiple_of(i * 16, 16), 16)
             out_ref[part] = (
@@ -683,14 +692,14 @@
 
     @pl.when(inner)
     def _():
+        for r in range(2):
+            await_bytes(extra_ref.at[pieces[r]], partial_sem.at[1 + r])
+            finish(lambda part: projected[part] + extra_ref[part].astype(jnp.float32), pieces[r])
         await_bytes(dense, partial_sem.at[0])
-        await_bytes(extra_ref, partial_sem.at[1])
-
-        finish(lambda part: projected[part] + extra_ref[part].astype(jnp.float32))
 
     @pl.when(outer)
     def _():
-        finish(lambda part: projected[part])
+        finish(lambda part: projected[part], slice(0, rows))
 
 
 def layer(
@@ -737,16 +746,14 @@
             pltpu.VMEM((rows, features), f32),
             pltpu.VMEM((rows, features), bf16),
             pltpu.VMEM((2, slots, rows), bf16),
-            pltpu.VMEM((2, rows, slots), bf16),
-            pltpu.VMEM((2, rows, slots), bf16),
+            pltpu.VMEM((2, 2 * rows, slots), bf16),
             pltpu.VMEM(gate.shape, bf16),
             pltpu.VMEM(up.shape, bf16),
             pltpu.VMEM(down.shape, bf16),
             pltpu.VMEM(routes.shape, jnp.int32),
             pltpu.VMEM(shares.shape, f32),
             pltpu.VMEM((slots, rows), bf16),
-            pltpu.VMEM((rows, slots), bf16),
-            pltpu.VMEM((rows, slots), bf16),
+            pltpu.VMEM((2 * rows, slots), bf16),
             pltpu.VMEM((rows, features), bf16),
             pltpu.VMEM((rows, features), bf16),
             dma((10,)),
@@ -773,7 +780,7 @@
             dma((2,)),
             dma((2,)),
             dma((2,)),
-            dma((2,)),
+            dma((3,)),
             dma((len(groups),)),
             dma((2 * len(groups),)),
             pltpu.SemaphoreType.REGULAR,

time: 185 us -> 183 us (0.989)
  Pallas kernels: 183 us -> 181 us
where the time goes in v8:
time: 183 us; the launch traced here: 182 us
  Pallas kernels  181 us (99%)
    pallas_call x1, Pallas kernels, layer(): pl.pallas_call(functools.partial(layer_kernel, sp, dp, len(groups)), out_...  181 us

profile of v8, /device:TPU:16, one launch (start us, length us, event | category | flops | bytes accessed | tf_op | source)
XLA Modules:
  0.0 182.5 jit_solution(16510258960977056739)
XLA Ops:
  0.0 181.5 %shard_map.127 = bf16[128,4096]{1,0:T(8,128)(2,1)S(1)} custom-call(bf16[128,16,128]{2,1,0:T(8,128)(2,1)} %bitcast.22, bf16[128,16,128]{2,1,0:T(8,128)(2,1)} %bitcast.23, bf16[128,16,128]{2,1,0:T(8,128)(2,1)} %bitcast.24, bf16[2048,1024]{1,0:T(8,128)(2,1)} %refs_3_.1, bf16[128,4096]{1,0:T(8,128)(2,1)} %bitcast.21, f32[1,4096]{1,0:T(1,128)} %bitcast.25, ...), custom_call_target="tpu_custom_call" | custom-call | tf_op jit(solution)/shard_map/pallas_call | solution.py:719
  181.5 1.0 copy.15

commit v9 on v8

--- a/solution.py
+++ b/solution.py
@@ -324,9 +324,6 @@
         pass_on(j)
     follow_all(local_heads - 1)
     pass_on(PIECES - 1)
-    for copy in fetches:
-        copy.start()
-
     @pl.when(inner)
     def _():
         for note in notes:
@@ -467,6 +464,8 @@
     def _():
         lend(rows // 16 - 1).start()
 
+    for copy in fetches:
+        copy.start()
     features = projected.shape[1]
     tile = 512
 

time: 183 us -> 183 us (level)
  no operation moved by 1% of the time
where the time goes in v9:
time: 183 us; the launch traced here: 182 us
  Pallas kernels  181 us (99%)
    pallas_call x1, Pallas kernels, layer(): pl.pallas_call(functools.partial(layer_kernel, sp, dp, len(groups)), out_...  181 us

profile of v9, /device:TPU:16, one launch (start us, length us, event | category | flops | bytes accessed | tf_op | source)
XLA Modules:
  0.0 182.5 jit_solution(7700274979104521525)
XLA Ops:
  0.0 181.5 %shard_map.127 = bf16[128,4096]{1,0:T(8,128)(2,1)S(1)} custom-call(bf16[128,16,128]{2,1,0:T(8,128)(2,1)} %bitcast.22, bf16[128,16,128]{2,1,0:T(8,128)(2,1)} %bitcast.23, bf16[128,16,128]{2,1,0:T(8,128)(2,1)} %bitcast.24, bf16[2048,1024]{1,0:T(8,128)(2,1)} %refs_3_.1, bf16[128,4096]{1,0:T(8,128)(2,1)} %bitcast.21, f32[1,4096]{1,0:T(1,128)} %bitcast.25, ...), custom_call_target="tpu_custom_call" | custom-call | tf_op jit(solution)/shard_map/pallas_call | solution.py:718
  181.5 1.0 copy.15
